TPU v7x, 512 devices: a whole 4x8x8 slice. The times are simulated.
512 devices in a mesh: sp: 64 (over z, y), tp: 8 (over x, core).
Axes of the slice: x: 4, y: 8, z: 8, core: 2. Of those that a mesh axis runs over, the one named last changes fastest.
Arguments:
- activations: bfloat16 [16384, 2048], P('sp', 'tp'), may hold values from -170 to 170
- norm_gain: float32 [2048], replicated, may hold values from 0.1 to 1.9
- query_weight: bfloat16 [2048, 1536], P(None, 'tp'), may hold values from -0.125 to 0.125
- latent_weight: bfloat16 [2048, 512], P(None, 'tp'), may hold values from -0.125 to 0.125
- rope_key_weight: bfloat16 [2048, 64], replicated, may hold values from -0.125 to 0.125
- latent_gain: float32 [512], replicated, may hold values from 1.5 to 64
- expand_weight: bfloat16 [512, 2048], P(None, 'tp'), may hold values from -0.25 to 0.25
- gate_weight: bfloat16 [2048, 1024], P(None, 'tp'), may hold values from -0.125 to 0.125
- pre_weight: bfloat16 [2048, 1024], P(None, 'tp'), may hold values from -0.125 to 0.125
- value_weight: bfloat16 [2048, 1024], P(None, 'tp'), may hold values from -0.125 to 0.125
- conv_kernel: bfloat16 [3, 1024], P(None, 'tp'), may hold values from -3.5 to 3.5
- output_attend: bfloat16 [1024, 2048], P('tp'), may hold values from -0.1875 to 0.1875
- output_conv: bfloat16 [1024, 2048], P('tp'), may hold values from -0.125 to 0.125
Outputs:
- mixed: bfloat16 [16384, 2048], P(('sp', 'tp'))
- log_weight_sum: float32 [8, 16384], P('tp', 'sp')
All inputs are finite; a program needn't handle non-finite values.
Results may differ from a plain program's by a relative error of at most 0.035.
The roundings to bfloat16 on the way count: a program that leaves them out, or rounds other values in their place, can miss the bound.
Values may be sent and summed in bfloat16 or wider, within the bound.
A program may use at most 128 MiB of HBM per device.

v0:
```python
import math

import jax
import jax.numpy as jnp
from jax import lax
from jax.sharding import PartitionSpec as P

D = 2048
NOPE = 128
ROPE = 64
VDIM = 128
GRID_W = 64


EPSILON = 1e-06
ROPE_BASE = 10000.0


def with_halo(array, sides, width):
    for axis, dim in sides:
        peers, length = (lax.axis_size(axis), array.shape[dim])
        up = [(i, (i + 1) % peers) for i in range(peers - 1)]
        down = [(j, i) for i, j in up]
        last = lax.slice_in_dim(array, length - width, length, axis=dim)
        leading = lax.slice_in_dim(array, 0, width, axis=dim)
        before = lax.ppermute(last, axis, up)
        after = lax.ppermute(leading, axis, down)
        array = jnp.concatenate([before, array, after], axis=dim)
    return array


def from_everyone(array, axis):
    copies = jnp.broadcast_to(array, (lax.axis_size(axis), *array.shape))
    return lax.all_to_all(copies, axis, split_axis=0, concat_axis=0, tiled=True)


def in_order(pieces, dim):
    pieces = jnp.moveaxis(pieces, 0, dim)
    dims = pieces.shape
    return pieces.reshape(*dims[:dim], dims[dim] * dims[dim + 1], *dims[dim + 2 :])


def gathered_copies(array, axis, dim):
    pieces = from_everyone(array, axis)
    return in_order(pieces, dim)


def sent_together(arrays, axis, dim, along):
    widths = [a.shape[along] for a in arrays]
    both = jnp.concatenate(arrays, axis=along)
    result = lax.all_gather(both, axis, axis=dim, tiled=True)
    return tuple(jnp.split(result, [sum(widths[:k]) for k in range(1, len(widths))], axis=along))


def split_up(array, dim, peers):
    before, after = (array.shape[:dim], array.shape[dim + 1 :])
    return jnp.moveaxis(array.reshape(*before, peers, -1, *after), dim, 0)


def sent_and_summed(array, axis, dim):
    pieces = split_up(array, dim, lax.axis_size(axis))
    arrived = lax.all_to_all(pieces, axis, split_axis=0, concat_axis=0, tiled=True)
    return arrived.astype(jnp.float32).sum(axis=0)


def rotate(inputs, grid_rows, grid_cols):
    quarter = inputs.shape[-1] // 4
    inverse = ROPE_BASE ** (-jnp.arange(quarter, dtype=jnp.float32) / quarter)
    row_angle = (grid_rows[:, None] * inverse)[:, None, :]
    col_angle = (grid_cols[:, None] * inverse)[:, None, :]
    part_one = inputs[..., :quarter]
    part_two = inputs[..., quarter : 2 * quarter]
    part_three = inputs[..., 2 * quarter : 3 * quarter]
    part_four = inputs[..., 3 * quarter :]
    return jnp.concatenate(
        [
            part_one * jnp.cos(row_angle) - part_two * jnp.sin(row_angle),
            part_one * jnp.sin(row_angle) + part_two * jnp.cos(row_angle),
            part_three * jnp.cos(col_angle) - part_four * jnp.sin(col_angle),
            part_three * jnp.sin(col_angle) + part_four * jnp.cos(col_angle),
        ],
        axis=-1,
    )


def conv_branch(gate_proj, pre_proj, value_proj, conv_kernel):
    pre_mix = (pre_proj * value_proj).astype(jnp.bfloat16)
    padded = with_halo(pre_mix, (("sp", 0),), 1).astype(jnp.float32)
    kernel = conv_kernel.astype(jnp.float32)
    convolved = kernel[0] * padded[:-2] + kernel[1] * padded[1:-1] + kernel[2] * padded[2:]
    return (gate_proj * convolved).astype(jnp.bfloat16)


def body(
    activations,
    norm_gain,
    query_weight,
    latent_weight,
    rope_key_weight,
    latent_gain,
    expand_weight,
    gate_weight,
    pre_weight,
    value_weight,
    conv_kernel,
    output_attend,
    output_conv,
):
    tokens_here = activations.shape[0]
    query_cols = query_weight.shape[1]
    heads_here = query_cols // (NOPE + ROPE)
    latent_cols = latent_weight.shape[1]
    channels = gate_weight.shape[1]
    joined = jnp.concatenate(
        [query_weight, latent_weight, rope_key_weight, gate_weight, pre_weight, value_weight],
        axis=1,
    )
    piece_f32 = gathered_copies(activations, "tp", 1).astype(jnp.float32)
    scaled = (piece_f32 * norm_gain).astype(jnp.bfloat16)
    running = jnp.dot(scaled, joined, preferred_element_type=jnp.float32)
    partial_squares = jnp.sum(piece_f32 * piece_f32, axis=1, keepdims=True)
    running, folded_squares = (running, partial_squares)
    inv_rms = lax.rsqrt(folded_squares / D + EPSILON)
    projected = running * inv_rms
    latent_end = query_cols + latent_cols
    rope_end = latent_end + ROPE
    query_proj = projected[:, :query_cols]
    latent_proj = projected[:, query_cols:latent_end]
    rope_proj = projected[:, latent_end:rope_end]
    gate_proj = projected[:, rope_end : rope_end + channels]
    pre_proj = projected[:, rope_end + channels : rope_end + 2 * channels]
    value_proj = projected[:, rope_end + 2 * channels :]
    positions = lax.axis_index("sp") * tokens_here + jnp.arange(tokens_here, dtype=jnp.int32)
    grid_rows = (positions // GRID_W).astype(jnp.float32)
    grid_cols = (positions % GRID_W).astype(jnp.float32)
    query = query_proj.reshape(tokens_here, heads_here, NOPE + ROPE)
    query = jnp.concatenate(
        [query[..., :NOPE], rotate(query[..., NOPE:], grid_rows, grid_cols)], axis=-1
    )
    query = (query * (NOPE + ROPE) ** (-0.5)).astype(jnp.bfloat16)
    query_nope = query[..., :NOPE]
    query_rope = query[..., NOPE:]
    gathered = gathered_copies(latent_proj.astype(jnp.bfloat16), "tp", 1).astype(jnp.float32)
    latent = (
        gathered
        * lax.rsqrt(jnp.mean(gathered * gathered, axis=1, keepdims=True) + EPSILON)
        * latent_gain
    ).astype(jnp.bfloat16)
    expanded = jnp.dot(latent, expand_weight, preferred_element_type=jnp.float32).astype(
        jnp.bfloat16
    )
    rope_key = rotate(rope_proj[:, None, :], grid_rows, grid_cols)[:, 0].astype(jnp.bfloat16)
    starting = (
        jnp.full((heads_here, tokens_here), -jnp.inf, jnp.float32),
        jnp.zeros((heads_here, tokens_here), jnp.float32),
        jnp.zeros((tokens_here, heads_here, VDIM), jnp.float32),
    )
    key_piece, rope_piece = sent_together((expanded, rope_key), "sp", 0, 1)
    piece_rows = key_piece.shape[0]
    key_block = math.gcd(piece_rows, 1024)
    split_heads = key_piece.reshape(piece_rows, heads_here, NOPE + VDIM)

    def one_block(turn_index, state):
        row_max, row_sum, running_out = state
        offset = turn_index * key_block
        block_keys = lax.dynamic_slice_in_dim(split_heads, offset, key_block, 0)
        block_rope = lax.dynamic_slice_in_dim(rope_piece, offset, key_block, 0)
        scores = jnp.einsum(
            "thd,jhd->htj", query_nope, block_keys[..., :NOPE], preferred_element_type=jnp.float32
        )
        scores = scores + jnp.einsum(
            "thd,jd->htj", query_rope, block_rope, preferred_element_type=jnp.float32
        )
        new_max = jnp.maximum(row_max, jnp.max(scores, axis=-1))
        rescale = jnp.exp(row_max - new_max)
        weights = jnp.exp(scores - new_max[..., None])
        row_sum = row_sum * rescale + jnp.sum(weights, axis=-1)
        running_out = running_out * rescale.T[..., None] + jnp.einsum(
            "htj,jhd->thd",
            weights.astype(jnp.bfloat16),
            block_keys[..., NOPE:],
            preferred_element_type=jnp.float32,
        )
        return (new_max, row_sum, running_out)

    row_max, row_sum, running_out = lax.fori_loop(0, piece_rows // key_block, one_block, starting)
    attended = (
        (running_out / row_sum.T[..., None])
        .astype(jnp.bfloat16)
        .reshape(tokens_here, heads_here * VDIM)
    )
    log_weight_sum = row_max + jnp.log(row_sum)
    conv_mixed = conv_branch(gate_proj, pre_proj, value_proj, conv_kernel)
    mixed = sent_and_summed(
        (
            jnp.dot(attended, output_attend, preferred_element_type=jnp.float32)
            + jnp.dot(conv_mixed, output_conv, preferred_element_type=jnp.float32)
        ).astype(jnp.bfloat16),
        "tp",
        0,
    ).astype(jnp.bfloat16)
    return (mixed, log_weight_sum)


def solution(mesh):
    return jax.shard_map(
        body,
        mesh=mesh,
        in_specs=(
            P("sp", "tp"),
            P(),
            P(None, "tp"),
            P(None, "tp"),
            P(),
            P(),
            P(None, "tp"),
            P(None, "tp"),
            P(None, "tp"),
            P(None, "tp"),
            P(None, "tp"),
            P("tp", None),
            P("tp", None),
        ),
        out_specs=(P(("sp", "tp"), None), P("tp", "sp")),
        check_vma=False,
    )
```

profile of v0, /device:TPU:1, one launch (start us, length us, event | category | flops | bytes accessed | tf_op | source)
XLA Modules:
  0.0 272.6 jit_solution(6182226679660591424)
XLA Ops:
  9.4 10.3 %all-to-all-start = ((bf16[8,256,256]{1,2,0:T(8,128)(2,1)}), bf16[8,256,256]{1,2,0:T(8,128)(2,1)S(1)}, u32[]{:S(2)}, u32[]{:S(2)}) async-start(bf16[8,256,256]{1,2,0:T(8,128)(2,1)} %broadcast_in_dim.17), calls=%async_computation | async-start | bytes 2097152 | tf_op jit(solution)/shard_map/all_to_all | solution.py:34
  23.4 1.7 constant_dynamic-update-slice_fusion.4
  25.1 1.7 constant_dynamic-update-slice_fusion.3
  29.3 5.4 %all-to-all-done = bf16[8,256,256]{1,2,0:T(8,128)(2,1)S(1)} async-done(((bf16[8,256,256]{1,2,0:T(8,128)(2,1)}), bf16[8,256,256]{1,2,0:T(8,128)(2,1)S(1)}, u32[]{:S(2)}, u32[]{:S(2)}) %all-to-all-start) | async-done | bytes 1048608 | tf_op jit(solution)/shard_map/all_to_all | solution.py:34
  38.5 4.3 %all-to-all-start.1 = ((bf16[8,256,64]{1,2,0:T(8,128)(2,1)}), bf16[8,256,64]{1,2,0:T(8,128)(2,1)S(1)}, u32[]{:S(2)}, u32[]{:S(2)}) async-start(bf16[8,256,64]{1,2,0:T(8,128)(2,1)} %broadcast_in_dim.18), calls=%async_computation.1 | async-start | bytes 524288 | tf_op jit(solution)/shard_map/all_to_all | solution.py:34
  43.2 6.1 %all-to-all-done.1 = bf16[8,256,64]{1,2,0:T(8,128)(2,1)S(1)} async-done(((bf16[8,256,64]{1,2,0:T(8,128)(2,1)}), bf16[8,256,64]{1,2,0:T(8,128)(2,1)S(1)}, u32[]{:S(2)}, u32[]{:S(2)}) %all-to-all-start.1) | async-done | bytes 262176 | tf_op jit(solution)/shard_map/all_to_all | solution.py:34
  50.7 1.3 collective-permute-start
  52.0 1.3 collective-permute-start.1
  53.5 3.2 %collective-permute-done.1 = bf16[1,128]{0,1:T(8,128)(2,1)S(1)} collective-permute-done((bf16[1,128]{0,1:T(8,128)(2,1)S(1)}, bf16[1,128]{0,1:T(8,128)(2,1)S(1)}, u32[]{:S(2)}, u32[]{:S(2)}) %collective-permute-start.1) | collective-permute-done | bytes 288 | tf_op jit(solution)/shard_map/ppermute | solution.py:27
  56.8 104.7 %all-gather.2.cloned.1.call-done = bf16[16384,320]{0,1:T(8,128)(2,1)} async-done(((bf16[256,320]{0,1:T(8,128)(2,1)}), bf16[16384,320]{0,1:T(8,128)(2,1)}) %all-gather.2.cloned.1.call-update) | async-done | bytes 10485776 | tf_op jit(solution)/shard_map/all_gather | solution.py:51
  161.5 7.6 %slice_bitcast_fusion = bf16[16384,1,256]{0,2,1:T(8,128)(2,1)} fusion(bf16[16384,320]{0,1:T(8,128)(2,1)} %all-gather.2.cloned.1.call-done), kind=kLoop, calls=%fused_computation.25 | loop fusion | bytes 16777216 | tf_op jit(solution)/shard_map/reshape | solution.py:161
  169.1 3.0 %split.9 = bf16[16384,64]{0,1:T(8,128)(2,1)} slice(bf16[16384,320]{0,1:T(8,128)(2,1)} %all-gather.2.cloned.1.call-done), slice={[0:16384], [256:320]} | slice | bytes 4194304 | tf_op jit(solution)/shard_map/split | solution.py:52
  172.1 66.0 %while.18 = (s32[]{:T(128)}, f32[1,256]{1,0:T(1,128)S(1)}, f32[1,256]{1,0:T(1,128)S(1)}, f32[256,1,128]{0,2,1:T(8,128)S(1)}, bf16[16384,1,256]{0,2,1:T(8,128)(2,...) while((s32[]{:T(128)}, f32[1,256]{1,0:T(1,128)S(1)}, ...), condition=%wide.region_5.6_spmd.clone, body=%wide.region_2.5_spmd.clone.sunk | while | flops 169444608 | bytes 6275283 | solution.py:186
  173.4 1.3 fusion.79
  175.0 1.3 fusion.83
  176.3 1.3 convolution_bitcast_fusion.4
  179.1 1.3 fusion.83
  180.4 1.3 convolution_bitcast_fusion.4
  183.2 1.3 fusion.83
  184.5 1.3 convolution_bitcast_fusion.4
  187.3 1.3 fusion.83
  188.6 1.3 convolution_bitcast_fusion.4
  191.5 1.3 fusion.83
  192.8 1.3 convolution_bitcast_fusion.4
  195.6 1.3 fusion.83
  196.9 1.3 convolution_bitcast_fusion.4
  199.7 1.3 fusion.83
  201.0 1.3 convolution_bitcast_fusion.4
  203.8 1.3 fusion.83
  205.2 1.3 convolution_bitcast_fusion.4
  208.0 1.3 fusion.83
  209.3 1.3 convolution_bitcast_fusion.4
  212.1 1.3 fusion.83
  213.4 1.3 convolution_bitcast_fusion.4
  216.2 1.3 fusion.83
  217.5 1.3 convolution_bitcast_fusion.4
  220.3 1.3 fusion.83
  221.7 1.3 convolution_bitcast_fusion.4
  224.5 1.3 fusion.83
  225.8 1.3 convolution_bitcast_fusion.4
  228.6 1.3 fusion.83
  229.9 1.3 convolution_bitcast_fusion.4
  232.7 1.3 fusion.83
  234.0 1.3 convolution_bitcast_fusion.4
  236.8 1.3 fusion.83
  239.2 1.6 fusion.16
  240.8 9.2 %all-to-all-start.2 = ((bf16[8,32,2048]{2,1,0:T(8,128)(2,1)}), bf16[8,32,2048]{2,1,0:T(8,128)(2,1)S(1)}, u32[]{:S(2)}, u32[]{:S(2)}) async-start(bf16[8,32,2048]{2,1,0:T(8,128)(2,1)} %bitcast.13), calls=%async_computation.2 | async-start | bytes 2097152 | tf_op jit(solution)/shard_map/all_to_all | solution.py:62
  250.6 14.4 %all-to-all-done.2 = bf16[8,32,2048]{2,1,0:T(8,128)(2,1)S(1)} async-done(((bf16[8,32,2048]{2,1,0:T(8,128)(2,1)}), bf16[8,32,2048]{2,1,0:T(8,128)(2,1)S(1)}, u32[]{:S(2)}, u32[]{:S(2)}) %all-to-all-start.2) | async-done | bytes 1048608 | tf_op jit(solution)/shard_map/all_to_all | solution.py:62
  (146 shorter events, 40.8 us)
Async XLA Ops:
  7.2 231.0 %copy-start = (bf16[128,2048]{1,0:T(8,128)(2,1)S(1)}, bf16[128,2048]{1,0:T(8,128)(2,1)}, u32[]{:S(2)}) copy-start(bf16[128,2048]{1,0:T(8,128)(2,1)} %param.26) | copy-start | bytes 1572868
  7.2 12.5 %copy-start.1 = (bf16[2048,192]{0,1:T(8,128)(2,1)S(1)}, bf16[2048,192]{0,1:T(8,128)(2,1)}, u32[]{:S(2)}) copy-start(bf16[2048,192]{0,1:T(8,128)(2,1)} %param.17) | copy-start | bytes 2359300
  7.2 13.5 %copy-start.3 = (bf16[2048,128]{1,0:T(8,128)(2,1)S(1)}, bf16[2048,128]{1,0:T(8,128)(2,1)}, u32[]{:S(2)}) copy-start(bf16[2048,128]{1,0:T(8,128)(2,1)} %param.22) | copy-start | bytes 1572868
  9.4 25.3 %all-to-all-start = ((bf16[8,256,256]{1,2,0:T(8,128)(2,1)}), bf16[8,256,256]{1,2,0:T(8,128)(2,1)S(1)}, u32[]{:S(2)}, u32[]{:S(2)}) async-start(bf16[8,256,256]{1,2,0:T(8,128)(2,1)} %broadcast_in_dim.17), calls=%async_computation | async-start | bytes 2097152 | tf_op jit(solution)/shard_map/all_to_all | solution.py:34
  23.4 11.6 %copy-start.6 = (f32[2048]{0:T(1024)S(1)}, f32[2048]{0:T(1024)}, u32[]{:S(2)}) copy-start(f32[2048]{0:T(1024)} %param.16) | copy-start | bytes 24580
  34.7 1.8 copy-start.5
  36.5 12.9 %copy-start.7 = (f32[512]{0:T(512)S(1)}, f32[512]{0:T(512)}, u32[]{:S(2)}) copy-start(f32[512]{0:T(512)} %param.20) | copy-start | bytes 6148
  36.5 13.1 %copy-start.4 = (bf16[512,256]{1,0:T(8,128)(2,1)S(1)}, bf16[512,256]{1,0:T(8,128)(2,1)}, u32[]{:S(2)}) copy-start(bf16[512,256]{1,0:T(8,128)(2,1)} %param.21) | copy-start | bytes 786436
  37.4 13.2 %copy-start.8 = (bf16[3,128]{1,0:T(4,128)(2,1)S(1)}, bf16[3,128]{1,0:T(4,128)(2,1)}, u32[]{:S(2)}) copy-start(bf16[3,128]{1,0:T(4,128)(2,1)} %param.25) | copy-start | bytes 2308
  38.5 10.8 %all-to-all-start.1 = ((bf16[8,256,64]{1,2,0:T(8,128)(2,1)}), bf16[8,256,64]{1,2,0:T(8,128)(2,1)S(1)}, u32[]{:S(2)}, u32[]{:S(2)}) async-start(bf16[8,256,64]{1,2,0:T(8,128)(2,1)} %broadcast_in_dim.18), calls=%async_computation.1 | async-start | bytes 524288 | tf_op jit(solution)/shard_map/all_to_all | solution.py:34
  42.8 118.7 %all-gather.2.cloned.1.call-start = ((), (), s32[]{:S(2)}) async-start(), calls=%async_computation.3 | async-start | bytes 10649600 | tf_op jit(solution)/shard_map/all_gather | solution.py:51
  50.7 2.8 %collective-permute-start = (bf16[1,128]{0,1:T(8,128)(2,1)S(1)}, bf16[1,128]{0,1:T(8,128)(2,1)S(1)}, u32[]{:S(2)}, u32[]{:S(2)}) collective-permute-start(bf16[1,128]{0,1:T(8,128)(2,1)S(1)} %get-tuple-element.215), channel_id=1, source_target_pairs={{0,8},{8,16},{16,24},{24,32},{32,40},{40,48},{48,56},{56,64},{64,7... | collective-permute-start | bytes 776 | tf_op jit(solution)/shard_map/ppermute | solution.py:26
  52.0 4.7 %collective-permute-start.1 = (bf16[1,128]{0,1:T(8,128)(2,1)S(1)}, bf16[1,128]{0,1:T(8,128)(2,1)S(1)}, u32[]{:S(2)}, u32[]{:S(2)}) collective-permute-start(bf16[1,128]{0,1:T(8,128)(2,1)S(1)} %get-tuple-element.216), channel_id=1, source_target_pairs={{8,0},{16,8},{24,16},{32,24},{40,32},{48,40},{56,48},{64,56},{72,6... | collective-permute-start | bytes 776 | tf_op jit(solution)/shard_map/ppermute | solution.py:27
  238.2 1.0 copy-start.2
  240.8 24.2 %all-to-all-start.2 = ((bf16[8,32,2048]{2,1,0:T(8,128)(2,1)}), bf16[8,32,2048]{2,1,0:T(8,128)(2,1)S(1)}, u32[]{:S(2)}, u32[]{:S(2)}) async-start(bf16[8,32,2048]{2,1,0:T(8,128)(2,1)} %bitcast.13), calls=%async_computation.2 | async-start | bytes 2097152 | tf_op jit(solution)/shard_map/all_to_all | solution.py:62
Sparse Core Ops, SparseCore 0:
  50.7 110.8 all-gather.1
where the time goes:
time: 275 us; the launch traced here: 273 us
  waiting for transfers between devices  134 us (49%)
  matrix products  64.4 us (23%)
  starting transfers between devices  26.4 us (10%)
  local copies, waits for them, and re-layouts  25.1 us (9%)
  between operations  14.3 us (5%)
  other arithmetic  7.71 us (3%)
    all_gather x1, waiting for transfers between devices, sent_together(): result = lax.all_gather(both, axis, axis=dim, tiled=True)  105 us
    dot_general x16, matrix products, one_block(): jnp.einsum('htj,jhd->thd', weights.astype(jnp.bfloat16), block_keys[...,...  20.4 us
    dot_general x16, matrix products, one_block(): jnp.einsum('thd,jhd->htj', query_nope, block_keys[..., :NOPE], preferred_...  20.4 us
    dot_general x16, matrix products, one_block(): jnp.einsum('thd,jd->htj', query_rope, block_rope, preferred_element_type=...  20.4 us
    all_to_all x2, starting transfers between devices, from_everyone(): return lax.all_to_all(copies, axis, split_axis=0, concat_axis=0, tiled=True)  14.6 us
    all_to_all x1, waiting for transfers between devices, sent_and_summed(): lax.all_to_all(pieces, axis, split_axis=0, concat_axis=0, tiled=True)  14.4 us
    unnamed x29, local copies, waits for them, and re-layouts  11.7 us
    all_to_all x2, waiting for transfers between devices, from_everyone(): return lax.all_to_all(copies, axis, split_axis=0, concat_axis=0, tiled=True)  11.5 us
  transfers between devices with their start and end apart: 6, of which 5 were waited for; matrix products, arithmetic and copies ran while one was open for 4% of the time, Pallas kernels for 0%

commit v1 on v0

v1 whole, which is shorter than its diff:
```python
import functools

import jax
import jax.numpy as jnp
import numpy as np
from jax import lax
from jax.experimental import pallas as pl
from jax.experimental.pallas import tpu as pltpu
from jax.sharding import PartitionSpec as P

MESH = pl.DeviceIdType.MESH
F32 = jnp.float32
BF16 = jnp.bfloat16

D = 2048
NOPE = 128
ROPE = 64
GRID_W = 64
EPSILON = 1e-06
ROPE_BASE = 10000.0
RING = 8
NX = 4
T = 256
Q_ROWS, Q_CHUNKS = 384, 2
KV_ROWS, KV_CHUNKS = 640, 4
LOW = -3.0e38


def rotation_tables():
    inverse = (np.float32(ROPE_BASE) ** (-np.arange(16, dtype=np.float32) / np.float32(16))).astype(np.float32)
    quarter = np.arange(128) // 16 % 4
    freq = inverse[np.arange(128) % 16]
    sign = np.where(quarter % 2 == 0, -1.0, 1.0)

    def table(count, mask):
        angle = (np.arange(count, dtype=np.float32)[:, None] * freq[None, :]).astype(np.float32)
        angle = angle.astype(np.float64)
        return np.concatenate([np.cos(angle) * mask, np.sin(angle) * sign * mask], axis=1).astype(np.float32)

    return table(256, quarter < 2), table(GRID_W, quarter >= 2)


def lane_iota(rows):
    return lax.broadcasted_iota(jnp.int32, (rows, 128), 1)


def kernel(
    act_hbm, gain_hbm, qw_hbm, lw_hbm, rw_hbm, lgain_hbm, ew_hbm, gw_hbm, pw_hbm, vw_hbm, ck_hbm, oa_hbm, oc_hbm,
    rowtab_hbm, coltab_hbm,
    mixed_ref, lws_ref,
    act_all, gain, qw, lw, rw, lgain, ew, wcat, ck, wout, rowtab, coltab, acc, lat_all,
    q_all, qr_all, kv_all, kr_all, vt_all, stats, o_acc, o_send, o_recv, st_recv,
    halo_out, halo_in, cat, e_psend, e_precv, e_own, e_xsend, e_xrecv,
    load_sem, a_send, a_recv, l_send, l_recv, q_send, q_recv, kv_send, kv_recv, d_send, d_recv,
    h_send, h_recv, ep_send, ep_recv, ex_send, ex_recv,
):
    sp = lax.axis_index("sp")
    tp = lax.axis_index("tp")
    x, c = lax.div(tp, 2), lax.rem(tp, 2)
    z, y = lax.div(sp, RING), lax.rem(sp, RING)
    ka, qa = y + c * (z - y), z + c * (y - z)
    k_stride, q_stride = 1 + 7 * c, 8 - 7 * c

    def ring(pos, offset):
        return lax.rem(pos + (offset + RING), RING)

    def k_dev(offset):
        return (sp + (ring(ka, offset) - ka) * k_stride, tp)

    def q_dev(offset):
        return (sp + (ring(qa, offset) - qa) * q_stride, tp)

    def chip(offset):
        return lax.rem(x + offset, NX)

    def t_dev(xx, cc):
        return (sp, 2 * xx + cc)

    sends = []

    def remote(src, dst, send, recv, dev):
        return pltpu.make_async_remote_copy(
            src_ref=src, dst_ref=dst, send_sem=send, recv_sem=recv, device_id=dev, device_id_type=MESH
        )

    def push(src, dst, send, recv, dev):
        copy = remote(src, dst, send, recv, dev)
        copy.start()
        sends.append(copy)

    def arrived(dst, send, recv, dev):
        remote(dst, dst, send, recv, dev).wait_recv()

    loads = []
    for i, (src, dst) in enumerate(
        [
            (act_hbm, act_all.at[tp]),
            (qw_hbm, qw),
            (rw_hbm, rw),
            (lw_hbm, lw),
            (gw_hbm, wcat.at[:, pl.ds(256, 128)]),
            (pw_hbm, wcat.at[:, pl.ds(384, 128)]),
            (vw_hbm, wcat.at[:, pl.ds(512, 128)]),
            (gain_hbm, gain),
            (lgain_hbm, lgain),
            (rowtab_hbm, rowtab),
            (coltab_hbm, coltab),
            (ck_hbm, ck),
            (ew_hbm, ew),
            (oa_hbm, wout.at[pl.ds(0, 128), :]),
            (oc_hbm, wout.at[pl.ds(128, 128), :]),
        ]
    ):
        copy = pltpu.make_async_copy(src, dst, load_sem.at[i])
        copy.start()
        loads.append(copy)

    barrier = pltpu.get_barrier_semaphore()
    partners = [(sp, lax.rem(tp + k, 8)) for k in range(1, 8)]
    partners += [q_dev(k) for k in range(1, 8)] + [k_dev(1), k_dev(-1)]
    after, before = (lax.rem(sp + 1, 64), tp), (lax.rem(sp + 63, 64), tp)
    partners += [after, before]
    for dev in partners:
        pl.semaphore_signal(barrier, inc=1, device_id=dev, device_id_type=MESH)
    loads[0].wait()
    pl.semaphore_wait(barrier, len(partners))

    def half(slot, h):
        return act_all.at[slot, pl.ds(128 * h, 128), :]

    count = [0]

    def a_push(slot, h, dev):
        push(half(slot, h), half(slot, h), a_send.at[count[0]], a_recv.at[slot, h], dev)
        count[0] += 1

    def a_wait(slot, h):
        arrived(half(slot, h), a_send.at[0], a_recv.at[slot, h], t_dev(x, 1 - c))

    up, down, mate = t_dev(chip(1), c), t_dev(chip(3), c), t_dev(x, 1 - c)
    a_push(tp, 0, up)
    a_push(tp, 1, down)
    a_push(tp, 0, mate)
    a_push(tp, 1, mate)
    a_push(tp, 1, up)
    a_push(tp, 0, down)

    for copy in loads[1:8]:
        copy.wait()

    def assemble(i, _):
        rows = pl.ds(i * 256, 256)
        wcat[rows, 0:128] = qw[rows, 0:128]
        wcat[rows, 128:256] = jnp.concatenate([qw[rows, 128:192], rw[rows, :]], axis=1)
        wcat[rows, 640:768] = jnp.concatenate([lw[rows, :], lw[rows, :]], axis=1)
        return 0

    lax.fori_loop(0, D // 256, assemble, 0)

    def project(slot, first):
        piece = act_all[slot].astype(F32)
        scaled = (piece * gain[:, pl.ds(pl.multiple_of(slot * 256, 256), 256)]).astype(BF16)
        part = jnp.dot(scaled, wcat[pl.ds(pl.multiple_of(slot * 256, 256), 256), :], preferred_element_type=F32)
        acc[...] = part if first else acc[...] + part
        squares = piece * piece
        return squares[:, 0:128] + squares[:, 128:256]

    squares = project(tp, True)
    s_down, s_up, s_far = 2 * chip(3) + c, 2 * chip(1) + c, 2 * chip(2) + c
    other = 1 - 2 * c
    a_wait(s_down, 0)
    a_push(s_down, 0, up)
    a_push(s_down, 0, mate)
    a_wait(s_up, 1)
    a_push(s_up, 1, down)
    a_push(s_up, 1, mate)
    for h in range(2):
        a_wait(tp + other, h)
    squares += project(tp + other, False)
    a_wait(s_down, 1)
    a_push(s_down, 1, mate)
    a_wait(s_up, 0)
    a_push(s_up, 0, mate)
    squares += project(s_down, False)
    squares += project(s_up, False)
    for slot in (s_down, s_up):
        for h in range(2):
            a_wait(slot + other, h)
        squares += project(slot + other, False)
    for h in range(2):
        a_wait(s_far, h)
        a_push(s_far, h, mate)
    squares += project(s_far, False)
    for h in range(2):
        a_wait(s_far + other, h)
    squares += project(s_far + other, False)
    inv_rms = lax.rsqrt(jnp.sum(squares, axis=1, keepdims=True) / D + EPSILON)

    low = lane_iota(128) < 64
    latent_part = acc[:, 640:768] * inv_rms
    lat_all[tp] = jnp.where(low, latent_part[0:128], latent_part[128:256]).astype(BF16)

    def l_push(i, slot, dev):
        push(lat_all.at[slot], lat_all.at[slot], l_send.at[i], l_recv.at[slot], dev)

    def l_wait(slot):
        arrived(lat_all.at[slot], l_send.at[0], l_recv.at[slot], mate)

    for i, dev in enumerate((t_dev(chip(2), c), up, down, mate)):
        l_push(i, tp, dev)

    for copy in loads[8:]:
        copy.wait()
    scale = (NOPE + ROPE) ** (-0.5)
    q_all[qa, 0:256, :] = (acc[:, 0:128] * inv_rms * scale).astype(BF16)
    raw = acc[:, 128:256] * inv_rms
    even = lax.rem(lax.div(lane_iota(T), 16), 2) == 0
    tables = [rowtab[pl.ds(sp * 4 + g, 1), :] + coltab[...] for g in range(4)]
    tables = jnp.concatenate(tables, axis=0)
    turned = jnp.where(even, pltpu.roll(raw, 112, 1), pltpu.roll(raw, 16, 1))
    rotated = raw * tables[:, 0:128] + turned * tables[:, 128:256]
    swapped = pltpu.roll(rotated, 64, 1)
    q_all[qa, 256:384, :] = (jnp.where(low, rotated[0:128], swapped[128:256]) * scale).astype(BF16)

    def chunks_of(direction, step, chunks):
        if step < 4:
            return range(chunks)
        return range(chunks // 2) if direction == 1 else range(chunks // 2, chunks)

    def ring_push(blocks, pos, rows, chunks, send, recv, dev, step):
        n = rows // chunks
        for ch in range(chunks):
            for d in (1, -1):
                if ch in chunks_of(d, step + 1, chunks):
                    part = blocks.at[ring(pos, -d * step), pl.ds(ch * n, n), :]
                    push(part, part, send.at[(1 - d) // 2, step, ch], recv.at[ring(pos, -d * step), ch], dev(d))

    def ring_step(blocks, pos, rows, chunks, send, recv, dev, step, ch):
        n = rows // chunks
        for d in (1, -1):
            if ch in chunks_of(d, step, chunks):
                slot = ring(pos, -d * step)
                part = blocks.at[slot, pl.ds(ch * n, n), :]
                arrived(part, send.at[0, 0, 0], recv.at[slot, ch], dev(d))
                if step < 4 and ch in chunks_of(d, step + 1, chunks):
                    push(part, part, send.at[(1 - d) // 2, step, ch], recv.at[slot, ch], dev(d))

    q_ring = (q_all, qa, Q_ROWS, Q_CHUNKS, q_send, q_recv, q_dev)
    kv_ring = (kv_all, ka, KV_ROWS, KV_CHUNKS, kv_send, kv_recv, k_dev)
    ring_push(*q_ring, 0)

    def open_query(slot):
        paired = q_all[slot, 256:384, :].astype(F32)
        qr_all[slot, 0:128, :] = jnp.where(low, paired, 0.0).astype(BF16)
        qr_all[slot, 128:256, :] = jnp.where(low, pltpu.roll(paired, 64, 1), 0.0).astype(BF16)

    def open_keys(slot):
        paired = kv_all[slot, 256:384, :]
        kr_all[slot, 0:128, :] = paired
        kr_all[slot, 128:256, :] = pltpu.roll(paired.astype(F32), 64, 1).astype(BF16)
        vt_all[slot] = jnp.transpose(kv_all[slot, 384:640, :].astype(F32)).astype(BF16)

    pre_mix = (acc[:, 384:512] * inv_rms) * (acc[:, 512:640] * inv_rms)
    pre_mix = pre_mix.astype(BF16).astype(F32)
    halo_out[0] = pre_mix[0:8]
    halo_out[1] = pre_mix[248:256]
    push(halo_out.at[0], halo_in.at[1], h_send.at[0], h_recv.at[1], before)
    push(halo_out.at[1], halo_in.at[0], h_send.at[1], h_recv.at[0], after)
    gate = acc[:, 256:384] * inv_rms

    kv_rope = jnp.where(low, swapped[0:128], rotated[128:256]).astype(BF16)
    kv_all[ka, 256:384, :] = kv_rope
    open_query(qa)
    stats[:, 0:1, :] = jnp.full((8, 1, T), LOW, F32)
    stats[:, 1:8, :] = jnp.zeros((8, 7, T), F32)
    o_acc[...] = jnp.zeros_like(o_acc)
    for i, slot in enumerate((s_down, s_up, s_far)):
        l_wait(slot)
        l_push(4 + i, slot, mate)
    for slot in (tp, s_down, s_up, s_far):
        l_wait_slot = slot + other
        l_wait(l_wait_slot)

    def pair(j):
        a, b = lat_all[2 * j].astype(F32), lat_all[2 * j + 1].astype(F32)
        return jnp.concatenate(
            [jnp.where(low, a, pltpu.roll(b, 64, 1)), jnp.where(low, pltpu.roll(a, 64, 1), b)], axis=0
        )

    parts = jnp.concatenate([pair(j) for j in range(4)], axis=1)
    latent_inv = lax.rsqrt(jnp.mean(parts * parts, axis=1, keepdims=True) + EPSILON)
    latent = (parts * latent_inv * lgain[...]).astype(BF16)
    expanded = jnp.dot(latent, ew[...], preferred_element_type=F32).astype(BF16)
    kv_all[ka, 0:256, :] = expanded[:, 0:128]
    kv_all[ka, 384:640, :] = expanded[:, 128:256]
    ring_push(*kv_ring, 0)

    for i in range(2):
        arrived(halo_in.at[i], h_send.at[0], h_recv.at[i], after)
    row = lax.broadcasted_iota(jnp.int32, (T, 128), 0)
    first = jnp.where(sp > 0, halo_in[0, 7:8, :], 0.0)
    last = jnp.where(sp < 63, halo_in[1, 0:1, :], 0.0)
    shifted_down = jnp.where(row == 0, first, pltpu.roll(pre_mix, 1, 0))
    shifted_up = jnp.where(row == T - 1, last, pltpu.roll(pre_mix, T - 1, 0))
    taps = ck[...].astype(F32)
    convolved = taps[0:1] * shifted_down + taps[1:2] * pre_mix + taps[2:3] * shifted_up
    cat[:, 128:256] = (gate * convolved).astype(BF16)
    open_keys(ka)

    def unit(qs, k, last_block):
        keys = jnp.concatenate([kv_all[k, 0:256, :], kr_all[k]], axis=1)
        values = vt_all[k]
        results = []
        for q in qs:
            queries = jnp.concatenate([q_all[q, 0:256, :], qr_all[q]], axis=1)
            scores = lax.dot_general(keys, queries, (((1,), (1,)), ((), ())), preferred_element_type=F32)
            old_max, old_sum = stats[q, 0:1, :], stats[q, 1:2, :]
            new_max = jnp.maximum(old_max, jnp.max(scores, axis=0, keepdims=True))
            rescale = jnp.exp(old_max - new_max)
            weights = jnp.exp(scores - new_max)
            new_sum = old_sum * rescale + jnp.sum(weights, axis=0, keepdims=True)
            out = jnp.dot(values, weights.astype(BF16), preferred_element_type=F32)
            results.append((new_max, new_sum, o_acc[q] * rescale + out))
        for q, (new_max, new_sum, out) in zip(qs, results):
            stats[q, 0:1, :] = new_max
            stats[q, 1:2, :] = new_sum
            o_acc[q] = out
            if last_block:
                o_send[q] = out.astype(BF16)

    def q_pair(p):
        return ring(qa, p), lax.rem(qa + RING - lax.rem(p, 4), RING)

    def units(pairs, keys):
        p0, pn = pairs
        k0, dk, kn = keys

        def step(i, _):
            p = p0 + lax.rem(i, pn)
            unit(q_pair(p), ring(ka, k0 + dk * lax.div(i, pn) + RING), False)
            return 0

        lax.fori_loop(0, pn * kn, step, 0)

    def q_step(step):
        for ch in range(Q_CHUNKS):
            ring_step(*q_ring, step, ch)
        for slot in {1: (ring(qa, step), ring(qa, -step))}.get(int(step < 4), (ring(qa, 4),)):
            open_query(slot)

    def kv_step(step):
        for ch in range(KV_CHUNKS):
            ring_step(*kv_ring, step, ch)
        for slot in {1: (ring(ka, step), ring(ka, -step))}.get(int(step < 4), (ring(ka, 4),)):
            open_keys(slot)

    q_step(1)
    units((1, 1), (0, 1, 1))
    q_step(2)
    kv_step(1)
    units((2, 1), (0, 1, 1))
    units((1, 2), (-1, 2, 2))
    q_step(3)
    units((3, 1), (-1, 1, 3))
    kv_step(2)
    units((1, 3), (-2, 4, 2))
    q_step(4)
    units((4, 1), (-2, 1, 5))
    kv_step(3)
    units((1, 4), (-3, 6, 2))
    kv_step(4)

    def d_push(offset):
        slot = ring(qa, offset)
        push(o_send.at[slot], o_recv.at[qa], d_send.at[offset, 0], d_recv.at[qa, 0], q_dev(offset))
        push(stats.at[slot], st_recv.at[qa], d_send.at[offset, 1], d_recv.at[qa, 1], q_dev(offset))

    for p in (4, 3, 2, 1):
        unit(q_pair(p), ring(ka, 4), True)
        d_push(p)
        if p < 4:
            d_push(8 - p)
    for offset in range(1, 8):
        slot = ring(qa, offset)
        arrived(o_recv.at[slot], d_send.at[1, 0], d_recv.at[slot, 0], q_dev(offset))
        arrived(st_recv.at[slot], d_send.at[1, 1], d_recv.at[slot, 1], q_dev(offset))
    whole_max = stats[qa, 0:1, :]
    for offset in range(1, 8):
        whole_max = jnp.maximum(whole_max, st_recv[ring(qa, offset), 0:1, :])
    weight = jnp.exp(stats[qa, 0:1, :] - whole_max)
    whole_sum = stats[qa, 1:2, :] * weight
    whole_out = o_acc[qa] * weight
    for offset in range(1, 8):
        slot = ring(qa, offset)
        weight = jnp.exp(st_recv[slot, 0:1, :] - whole_max)
        whole_sum += st_recv[slot, 1:2, :] * weight
        whole_out += o_recv[slot].astype(F32) * weight
    lws_ref[...] = whole_max + jnp.log(whole_sum)
    cat[:, 0:128] = jnp.transpose(whole_out / whole_sum).astype(BF16)

    def rows_of(xx, cc):
        return pl.ds(pl.multiple_of((2 * xx + cc) * 32, 32), 32)

    order = [chip(2), chip(1), chip(3), x]
    for_mate = jnp.concatenate([cat[rows_of(xx, 1 - c), :] for xx in order], axis=0)
    for n in range(4):
        cols = slice(512 * n, 512 * n + 512)
        part = jnp.dot(for_mate, wout[:, cols], preferred_element_type=F32).astype(BF16)
        for j in range(4):
            e_psend[j, :, cols] = part[32 * j : 32 * j + 32]
    for j in range(4):
        push(e_psend.at[j], e_precv.at[j], ep_send.at[j], ep_recv.at[j], mate)
    for_own = jnp.concatenate([cat[rows_of(xx, c), :] for xx in order], axis=0)
    for n in range(4):
        cols = slice(512 * n, 512 * n + 512)
        part = jnp.dot(for_own, wout[:, cols], preferred_element_type=F32)
        for j in range(4):
            e_own[j, :, cols] = part[32 * j : 32 * j + 32]
    for j in range(3):
        arrived(e_precv.at[j], ep_send.at[0], ep_recv.at[j], mate)
        e_xsend[j] = (e_own[j] + e_precv[j].astype(F32)).astype(BF16)
        push(e_xsend.at[j], e_xrecv.at[j], ex_send.at[j], ex_recv.at[j], t_dev(order[j], c))
    arrived(e_precv.at[3], ep_send.at[0], ep_recv.at[3], mate)
    total = e_own[3] + e_precv[3].astype(F32)
    for j in (1, 2, 0):
        arrived(e_xrecv.at[j], ex_send.at[0], ex_recv.at[j], t_dev(order[j], c))
        total += e_xrecv[j].astype(F32)
    mixed_ref[...] = total.astype(BF16)
    for copy in sends:
        copy.wait_send()


def body(
    activations, norm_gain, query_weight, latent_weight, rope_key_weight, latent_gain, expand_weight,
    gate_weight, pre_weight, value_weight, conv_kernel, output_attend, output_conv,
):
    rowtab, coltab = rotation_tables()
    dma = pltpu.SemaphoreType.DMA
    vmem = pltpu.VMEM
    return pl.pallas_call(
        kernel,
        out_shape=(jax.ShapeDtypeStruct((32, D), BF16), jax.ShapeDtypeStruct((1, T), F32)),
        in_specs=[pl.BlockSpec(memory_space=pl.ANY)] * 15,
        out_specs=(pl.BlockSpec(memory_space=vmem), pl.BlockSpec(memory_space=vmem)),
        scratch_shapes=[
            vmem((8, T, 256), BF16),
            vmem((1, D), F32),
            vmem((D, 192), BF16),
            vmem((D, 64), BF16),
            vmem((D, 64), BF16),
            vmem((1, 512), F32),
            vmem((512, 256), BF16),
            vmem((D, 768), BF16),
            vmem((3, 128), BF16),
            vmem((256, D), BF16),
            vmem((256, 256), F32),
            vmem((64, 256), F32),
            vmem((T, 768), F32),
            vmem((8, 128, 128), BF16),
            vmem((8, Q_ROWS, 128), BF16),
            vmem((8, T, 128), BF16),
            vmem((8, KV_ROWS, 128), BF16),
            vmem((8, T, 128), BF16),
            vmem((8, 128, T), BF16),
            vmem((8, 8, T), F32),
            vmem((8, 128, T), F32),
            vmem((8, 128, T), BF16),
            vmem((8, 128, T), BF16),
            vmem((8, 8, T), F32),
            vmem((2, 8, 128), F32),
            vmem((2, 8, 128), F32),
            vmem((T, 256), BF16),
            vmem((4, 32, D), BF16),
            vmem((4, 32, D), BF16),
            vmem((4, 32, D), F32),
            vmem((3, 32, D), BF16),
            vmem((3, 32, D), BF16),
            dma((15,)),
            dma((14,)),
            dma((8, 2)),
            dma((7,)),
            dma((8,)),
            dma((2, 4, Q_CHUNKS)),
            dma((8, Q_CHUNKS)),
            dma((2, 4, KV_CHUNKS)),
            dma((8, KV_CHUNKS)),
            dma((8, 2)),
            dma((8, 2)),
            dma((2,)),
            dma((2,)),
            dma((4,)),
            dma((4,)),
            dma((3,)),
            dma((3,)),
        ],
        compiler_params=pltpu.CompilerParams(collective_id=0, has_side_effects=True),
    )(
        activations, norm_gain.reshape(1, D), query_weight, latent_weight, rope_key_weight,
        latent_gain.reshape(1, 512), expand_weight, gate_weight, pre_weight, value_weight, conv_kernel,
        output_attend, output_conv, jnp.asarray(rowtab), jnp.asarray(coltab),
    )


def solution(mesh):
    return jax.shard_map(
        body,
        mesh=mesh,
        in_specs=(
            P("sp", "tp"),
            P(),
            P(None, "tp"),
            P(None, "tp"),
            P(),
            P(),
            P(None, "tp"),
            P(None, "tp"),
            P(None, "tp"),
            P(None, "tp"),
            P(None, "tp"),
            P("tp", None),
            P("tp", None),
        ),
        out_specs=(P(("sp", "tp"), None), P("tp", "sp")),
        check_vma=False,
    )
```

time: 275 us -> 87.1 us (0.32)
  waiting for transfers between devices: 134 us -> 0 us
  Pallas kernels: 0 us -> 78.8 us
  matrix products: 64.4 us -> 0 us
  starting transfers between devices: 26.4 us -> 0 us
  local copies, waits for them, and re-layouts: 25.1 us -> 7.42 us
  between operations: 14.3 us -> 0.66 us
  other arithmetic: 7.71 us -> 0 us
    all_gather x1 -> x0, waiting for transfers between devices: 105 us -> none  [sent_together(): result = lax.all_gather(both, axis, axis=dim, tiled=True)]
    pallas_call x0 -> x1, Pallas kernels: none -> 78.8 us  [body(): pl.pallas_call(kernel, out_shape=(jax.ShapeDtypeStruct((32, D), BF16), ja...]
    dot_general x52 -> x0, matrix products: 64.4 us -> none  [the longest x16 20.4 us: one_block(): jnp.einsum('htj,jhd->thd', weights.astype(jnp.bfloat16), block_keys[...,...]
    all_to_all x3 -> x0, waiting for transfers between devices: 25.9 us -> none  [the longest x1 14.4 us: sent_and_summed(): lax.all_to_all(pieces, axis, split_axis=0, concat_axis=0, tiled=True)]
    all_to_all x3 -> x0, starting transfers between devices: 23.8 us -> none  [the longest x2 14.6 us: from_everyone(): return lax.all_to_all(copies, axis, split_axis=0, concat_axis=0, tiled=True)]
    reshape x2 -> x0, local copies, waits for them, and re-layouts: 7.59 us -> none  [the longest x1 7.58 us: body(): split_heads = key_piece.reshape(piece_rows, heads_here, NOPE + VDIM)]
    reduce_sum x19 -> x0, other arithmetic: 4.77 us -> none  [the longest x16 3.55 us: one_block(): row_sum = row_sum * rescale + jnp.sum(weights, axis=-1)]
    unnamed x29 -> x9, local copies, waits for them, and re-layouts: 11.7 us -> 7.42 us
  transfers between devices with their start and end apart: 6 -> 0, of which waited for: 5 -> 0; matrix products, arithmetic and copies ran while one was open for 4% -> 0% of each run, Pallas kernels for 0% -> 0%
where the time goes in v1:
time: 87.1 us; the launch traced here: 86.9 us
  Pallas kernels  78.8 us (90%)
  local copies, waits for them, and re-layouts  7.42 us (9%)
    pallas_call x1, Pallas kernels, body(): pl.pallas_call(kernel, out_shape=(jax.ShapeDtypeStruct((32, D), BF16), ja...  78.8 us
    unnamed x9, local copies, waits for them, and re-layouts  7.42 us

profile of v1, /device:TPU:1, one launch (start us, length us, event | category | flops | bytes accessed | tf_op | source)
XLA Modules:
  0.0 86.9 jit_solution(10858300069250159101)
XLA Ops:
  0.6 0.0 copy-start
  0.6 2.0 %copy.18.lw_hbm = bf16[2048,64]{1,0:T(8,128)(2,1)} copy(bf16[2048,64]{0,1:T(8,128)(2,1)} %param.18) | data formatting | bytes 524288 | tf_op args[3]
  2.7 2.0 %copy.19.rw_hbm = bf16[2048,64]{1,0:T(8,128)(2,1)} copy(bf16[2048,64]{0,1:T(8,128)(2,1)} %param.19) | data formatting | bytes 524288 | tf_op args[4]
  4.6 0.0 copy-done
  4.6 1.3 %copy.17.qw_hbm = bf16[2048,192]{1,0:T(8,128)(2,1)} copy(bf16[2048,192]{0,1:T(8,128)(2,1)S(1)} %copy-done) | data formatting | bytes 1572864 | tf_op args[2]
  5.9 78.8 %shard_map.158 = (bf16[32,2048]{1,0:T(8,128)(2,1)}, f32[1,256]{1,0:T(1,128)}) custom-call(bf16[256,256]{1,0:T(8,128)(2,1)} %act_hbm.1, f32[1,2048]{1,0:T(1,128)} %bitcast.2, bf16[2048,192]{1,0:T(8,128)(2,1)} %copy.17.qw_hbm, bf16[2048,64]{1,0:T(8,128)(2,1)} %copy.18.lw_hbm, bf16[2048,64]{1,0:T(8,128)(2,1)} %copy.19.rw_hbm, f32[1,512]{1,0:T(1,128)} %bitcast.3, ...), custom_call_target="tpu_custom_call" | custom-call | tf_op jit(solution)/shard_map/pallas_call | solution.py:440
  84.8 0.0 copy-start.1
  84.8 1.6 %copy.22 = bf16[32,2048]{1,0:T(8,128)(2,1)} copy(bf16[32,2048]{1,0:T(8,128)(2,1)} %get-tuple-element.4) | data formatting | bytes 262144
  86.3 0.0 copy-done.1
  86.3 0.6 copy.23
Async XLA Ops:
  0.6 4.0 %copy-start = (bf16[2048,192]{0,1:T(8,128)(2,1)S(1)}, bf16[2048,192]{0,1:T(8,128)(2,1)}, u32[]{:S(2)}) copy-start(bf16[2048,192]{0,1:T(8,128)(2,1)} %param.17) | copy-start | bytes 2359300
  84.8 1.6 %copy-start.1 = (f32[1,256]{1,0:T(1,128)S(1)}, f32[1,256]{1,0:T(1,128)}, u32[]{:S(2)}) copy-start(f32[1,256]{1,0:T(1,128)} %get-tuple-element.5) | copy-start | bytes 3076

commit v2 on v1

v2 whole, which is shorter than its diff:
```python
import functools

import jax
import jax.numpy as jnp
import numpy as np
from jax import lax
from jax.experimental import pallas as pl
from jax.experimental.pallas import tpu as pltpu
from jax.sharding import PartitionSpec as P

MESH = pl.DeviceIdType.MESH
F32 = jnp.float32
BF16 = jnp.bfloat16

D = 2048
NOPE = 128
ROPE = 64
GRID_W = 64
EPSILON = 1e-06
ROPE_BASE = 10000.0
RING = 8
NX = 4
T = 256
Q_ROWS = 384
KV_ROWS, KV_CHUNKS = 640, 4
V_ROWS = 144
LOW = -3.0e38
LOG2E = 1.4426950408889634


def rotation_tables():
    inverse = (np.float32(ROPE_BASE) ** (-np.arange(16, dtype=np.float32) / np.float32(16))).astype(np.float32)
    quarter = np.arange(128) // 16 % 4
    freq = inverse[np.arange(128) % 16]
    sign = np.where(quarter % 2 == 0, -1.0, 1.0)

    def table(count, mask):
        angle = (np.arange(count, dtype=np.float32)[:, None] * freq[None, :]).astype(np.float32)
        angle = angle.astype(np.float64)
        return np.concatenate([np.cos(angle) * mask, np.sin(angle) * sign * mask], axis=1).astype(np.float32)

    return np.concatenate([table(256, quarter < 2), table(GRID_W, quarter >= 2)])


def lane_iota(rows):
    return lax.broadcasted_iota(jnp.int32, (rows, 128), 1)


def kernel(
    act_hbm, gain_hbm, qw_hbm, lw_hbm, rw_hbm, lgain_hbm, ew_hbm, gw_hbm, pw_hbm, vw_hbm, ck_hbm, oa_hbm, oc_hbm,
    table_hbm,
    mixed_ref, lws_ref,
    act_all, gain, lgain, ew, wt, wb, ck, wout, table, acc, acc_b, lat_all,
    q_all, q_cat, kv_all, k_cat, vt_all, s_buf, w_buf, r_buf, stats, o_acc, o_send, o_recv, st_recv,
    halo_out, halo_in, cat, e_psend, e_precv, e_own, e_xsend, e_xrecv,
    load_sem, sent, a_recv, l_recv, q_recv, kv_recv, d_recv, h_recv, ep_recv, ex_recv,
):
    sp = lax.axis_index("sp")
    tp = lax.axis_index("tp")
    x, c = lax.div(tp, 2), lax.rem(tp, 2)
    z, y = lax.div(sp, RING), lax.rem(sp, RING)
    ka, qa = y + c * (z - y), z + c * (y - z)
    k_stride, q_stride = 1 + 7 * c, 8 - 7 * c

    def ring(pos, offset):
        return lax.rem(pos + (offset + RING), RING)

    def k_dev(offset):
        return (sp + (ring(ka, offset) - ka) * k_stride, tp)

    def q_dev(offset):
        return (sp + (ring(qa, offset) - qa) * q_stride, tp)

    def chip(offset):
        return lax.rem(x + offset, NX)

    def t_dev(xx, cc):
        return (sp, 2 * xx + cc)

    scopes = []
    A, L, Q, KV, O, ST, EP, EX, H = (sent.at[i] for i in range(9))

    def phase(name):
        if scopes:
            scopes.pop().__exit__(None, None, None)
        if name:
            scopes.append(jax.named_scope(name))
            scopes[-1].__enter__()

    def remote(src, dst, send, recv, dev):
        return pltpu.make_async_remote_copy(
            src_ref=src, dst_ref=dst, send_sem=send, recv_sem=recv, device_id=dev, device_id_type=MESH
        )

    def push(src, dst, send, recv, dev):
        remote(src, dst, send, recv, dev).start()

    def arrived(bytes_of, recv):
        remote(bytes_of, bytes_of, A, recv, t_dev(x, 1 - c)).wait_recv()

    phase("loads")
    def load(i, *pairs):
        for src, dst in pairs:
            pltpu.make_async_copy(src, dst, load_sem.at[i]).start()

    def loaded(i, ref):
        pltpu.make_async_copy(ref, ref, load_sem.at[i]).wait()

    load(0, (act_hbm, act_all.at[tp]))
    load(1, (gain_hbm, gain))
    load(
        2,
        (qw_hbm, wt.at[pl.ds(0, 192), :]),
        (rw_hbm, wt.at[pl.ds(192, 64), :]),
        (lw_hbm, wt.at[pl.ds(256, 64), :]),
        (lw_hbm, wt.at[pl.ds(320, 64), :]),
    )
    load(
        3,
        (gw_hbm, wb.at[:, pl.ds(0, 128)]),
        (pw_hbm, wb.at[:, pl.ds(128, 128)]),
        (vw_hbm, wb.at[:, pl.ds(256, 128)]),
    )
    load(4, (lgain_hbm, lgain))
    load(5, (table_hbm, table))
    load(6, (ck_hbm, ck))
    load(7, (ew_hbm, ew))
    load(8, (oa_hbm, wout.at[pl.ds(0, 128), :]), (oc_hbm, wout.at[pl.ds(128, 128), :]))

    phase("barrier")
    barrier = pltpu.get_barrier_semaphore()
    partners = [(sp, lax.rem(tp + k, 8)) for k in range(1, 8)]
    partners += [q_dev(k) for k in range(1, 8)] + [k_dev(1), k_dev(-1)]
    after, before = (lax.rem(sp + 1, 64), tp), (lax.rem(sp + 63, 64), tp)
    partners += [after, before]
    for dev in partners:
        pl.semaphore_signal(barrier, inc=1, device_id=dev, device_id_type=MESH)
    loaded(0, act_all.at[tp])
    pl.semaphore_wait(barrier, len(partners))

    phase("act_own")
    def rows_at(slot, ch, n):
        return act_all.at[slot, pl.ds(64 * ch, 64 * n), :]

    def a_push(slot, ch, n, recv, dev):
        push(rows_at(slot, ch, n), rows_at(slot, ch, n), A, a_recv.at[recv], dev)

    def a_wait(n, recv):
        arrived(act_all.at[0, pl.ds(0, 64 * n), :], a_recv.at[recv])

    up, down, mate = t_dev(chip(1), c), t_dev(chip(3), c), t_dev(x, 1 - c)
    for i in range(2):
        a_push(tp, i, 1, i, up)
        a_push(tp, 2 + i, 1, 3 + i, down)
    a_push(tp, 0, 4, 7, mate)
    a_push(tp, 2, 2, 2, up)
    a_push(tp, 0, 2, 5, down)
    loaded(1, gain)
    loaded(2, wt)
    loaded(3, wb)

    def project(slot, first):
        piece = act_all[slot].astype(F32)
        features = pl.ds(pl.multiple_of(slot * 256, 256), 256)
        scaled = (piece * gain[:, features]).astype(BF16)
        part = lax.dot_general(scaled, wt[:, features], (((1,), (1,)), ((), ())), preferred_element_type=F32)
        acc[...] = part if first else acc[...] + part
        part = jnp.dot(scaled, wb[features, :], preferred_element_type=F32)
        acc_b[...] = part if first else acc_b[...] + part
        squares = piece * piece
        return squares[:, 0:128] + squares[:, 128:256]

    squares = project(tp, True)
    phase("act_one")
    s_down, s_up, s_far = 2 * chip(3) + c, 2 * chip(1) + c, 2 * chip(2) + c
    other = 1 - 2 * c
    for i in range(2):
        a_wait(1, i)
        a_push(s_down, i, 1, 6, up)
        a_wait(1, 3 + i)
        a_push(s_up, 2 + i, 1, 6, down)
    a_wait(2, 2)
    a_push(s_down, 0, 4, 8, mate)
    a_wait(2, 5)
    a_push(s_up, 0, 4, 9, mate)
    a_wait(4, 7)
    squares += project(tp + other, False)
    squares += project(s_down, False)
    squares += project(s_up, False)
    a_wait(4, 8)
    squares += project(s_down + other, False)
    a_wait(4, 9)
    squares += project(s_up + other, False)
    phase("act_far")
    a_wait(4, 6)
    a_push(s_far, 0, 4, 10, mate)
    squares += project(s_far, False)
    a_wait(4, 10)
    squares += project(s_far + other, False)
    phase("latent_send")
    inv_rms = lax.rsqrt(jnp.sum(squares, axis=1, keepdims=True) / D + EPSILON)

    low = lane_iota(128) < 64
    latent_part = acc[:, 256:384] * inv_rms
    lat_all[tp] = jnp.where(low, latent_part[0:128], latent_part[128:256]).astype(BF16)

    def l_push(slot, recv, dev):
        push(lat_all.at[slot], lat_all.at[slot], L, l_recv.at[recv], dev)

    for i, dev in enumerate((t_dev(chip(2), c), up, down, mate)):
        l_push(tp, i, dev)

    phase("query")
    loaded(4, lgain)
    loaded(5, table)
    loaded(6, ck)
    loaded(7, ew)
    loaded(8, wout)
    scale = (NOPE + ROPE) ** (-0.5) * LOG2E
    q_all[qa, 0:256, :] = (acc[:, 0:128] * inv_rms * scale).astype(BF16)
    raw = acc[:, 128:256] * inv_rms
    even = lax.rem(lax.div(lane_iota(T), 16), 2) == 0
    tables = [table[pl.ds(sp * 4 + g, 1), :] + table[256:320, :] for g in range(4)]
    tables = jnp.concatenate(tables, axis=0)
    turned = jnp.where(even, pltpu.roll(raw, 112, 1), pltpu.roll(raw, 16, 1))
    rotated = raw * tables[:, 0:128] + turned * tables[:, 128:256]
    swapped = pltpu.roll(rotated, 64, 1)
    q_all[qa, 256:384, :] = (jnp.where(low, rotated[0:128], swapped[128:256]) * scale).astype(BF16)

    def q_push(offset, ch, n, recv, to):
        part = q_all.at[ring(qa, offset), pl.ds(192 * ch, 192 * n), :]
        push(part, part, Q, q_recv.at[recv], q_dev(to))

    def q_wait(n, recv):
        arrived(q_all.at[pl.ds(0, n)] if n else q_all.at[0, pl.ds(0, 192), :], q_recv.at[recv])

    q_push(0, 0, 2, 0, 1)
    q_push(0, 0, 2, 1, -1)
    q_push(0, 0, 1, 2, 2)
    q_push(0, 1, 1, 3, -2)
    q_push(0, 1, 1, 4, 2)
    q_push(0, 0, 1, 4, -2)

    n_kv = KV_ROWS // KV_CHUNKS

    def kv_push(step, ch, to):
        part = kv_all.at[ring(ka, -to * step), pl.ds(ch * n_kv, n_kv), :]
        recv = step * KV_CHUNKS + ch if step < 3 else 3 * KV_CHUNKS
        push(part, part, KV, kv_recv.at[recv], k_dev(to))

    def kv_step(step, some):
        for ch in some:
            arrived(kv_all.at[0, pl.ds(0, 2 * n_kv), :], kv_recv.at[(step - 1) * KV_CHUNKS + ch])
            if step < 3 or ch < KV_CHUNKS // 2:
                kv_push(step, ch, 1)
            if step < 3 or ch >= KV_CHUNKS // 2:
                kv_push(step, ch, -1)

    def open_query(slot):
        paired = q_all[slot, 256:384, :].astype(F32)
        q_cat[slot, :, 0:128] = q_all[slot, 0:256, :]
        q_cat[slot, 0:128, 128:256] = jnp.where(low, paired, 0.0).astype(BF16)
        q_cat[slot, 128:256, 128:256] = jnp.where(low, pltpu.roll(paired, 64, 1), 0.0).astype(BF16)

    def open_keys(slot):
        paired = kv_all[slot, 256:384, :]
        k_cat[slot, :, 0:128] = kv_all[slot, 0:256, :]
        k_cat[slot, 0:128, 128:256] = paired
        k_cat[slot, 128:256, 128:256] = pltpu.roll(paired.astype(F32), 64, 1).astype(BF16)
        vt_all[slot, 0:128, :] = jnp.transpose(kv_all[slot, 384:640, :].astype(F32)).astype(BF16)

    phase("halo")
    pre_mix = (acc_b[:, 128:256] * inv_rms) * (acc_b[:, 256:384] * inv_rms)
    pre_mix = pre_mix.astype(BF16).astype(F32)
    halo_out[0] = pre_mix[0:8]
    halo_out[1] = pre_mix[248:256]
    push(halo_out.at[0], halo_in.at[1], H, h_recv.at[0], before)
    push(halo_out.at[1], halo_in.at[0], H, h_recv.at[0], after)
    gate = acc_b[:, 0:128] * inv_rms

    phase("latent_wait")
    kv_rope = jnp.where(low, swapped[0:128], rotated[128:256]).astype(BF16)
    kv_all[ka, 256:384, :] = kv_rope
    open_query(qa)
    stats[:, 0:1, :] = jnp.full((8, 1, T), LOW, F32)
    stats[:, 1:8, :] = jnp.zeros((8, 7, T), F32)
    o_acc[...] = jnp.zeros_like(o_acc)
    ones = lax.broadcasted_iota(jnp.int32, (8, V_ROWS - 128, T), 1) == 0
    vt_all[:, 128:V_ROWS, :] = jnp.where(ones, 1.0, 0.0).astype(BF16)
    phase("q1")
    q_wait(1, 0)
    q_push(-1, 0, 2, 5, 2)
    q_wait(1, 1)
    q_push(1, 0, 2, 5, -2)
    phase("latent_x")
    for recv, slot in ((1, s_down), (2, s_up), (0, s_far)):
        arrived(lat_all.at[0], l_recv.at[recv])
        l_push(slot, 3, mate)
    phase("q2")
    q_wait(0, 2)
    q_push(-2, 0, 1, 6, 2)
    q_wait(0, 3)
    q_push(2, 1, 1, 6, -2)
    phase("latent_mate")
    arrived(lat_all.at[pl.ds(0, 4)], l_recv.at[3])

    def pair(j):
        a, b = lat_all[2 * j].astype(F32), lat_all[2 * j + 1].astype(F32)
        return jnp.concatenate(
            [jnp.where(low, a, pltpu.roll(b, 64, 1)), jnp.where(low, pltpu.roll(a, 64, 1), b)], axis=0
        )

    phase("expand")
    parts = jnp.concatenate([pair(j) for j in range(4)], axis=1)
    latent_inv = lax.rsqrt(jnp.mean(parts * parts, axis=1, keepdims=True) + EPSILON)
    latent = (parts * latent_inv * lgain[...]).astype(BF16)
    expanded = jnp.dot(latent, ew[...], preferred_element_type=F32).astype(BF16)
    kv_all[ka, 0:256, :] = expanded[:, 0:128]
    kv_all[ka, 384:640, :] = expanded[:, 128:256]
    for ch in range(KV_CHUNKS):
        kv_push(0, ch, 1)
        kv_push(0, ch, -1)

    phase("conv")
    arrived(halo_in, h_recv.at[0])
    row = lax.broadcasted_iota(jnp.int32, (T, 128), 0)
    first = jnp.where(sp > 0, halo_in[0, 7:8, :], 0.0)
    last = jnp.where(sp < 63, halo_in[1, 0:1, :], 0.0)
    shifted_down = jnp.where(row == 0, first, pltpu.roll(pre_mix, 1, 0))
    shifted_up = jnp.where(row == T - 1, last, pltpu.roll(pre_mix, T - 1, 0))
    taps = ck[...].astype(F32)
    convolved = taps[0:1] * shifted_down + taps[1:2] * pre_mix + taps[2:3] * shifted_up
    cat[:, 128:256] = (gate * convolved).astype(BF16)
    open_keys(ka)

    phase("q_rest")
    first_chunks, other_chunks = range(KV_CHUNKS // 2), range(KV_CHUNKS // 2, KV_CHUNKS)
    q_wait(1, 4)
    for offset in (1, -1, 2, -2):
        open_query(ring(qa, offset))
    phase("q3")
    q_wait(2, 5)
    for offset in (3, -3):
        open_query(ring(qa, offset))
    phase("q4")
    q_wait(1, 6)
    open_query(ring(qa, 4))

    def key_blocks(ks, qs):
        n = len(ks) * T
        keys = jnp.concatenate([k_cat[k] for k in ks], axis=0)
        values = jnp.concatenate([vt_all[k] for k in ks], axis=1)
        for i, q in enumerate(qs):
            s_buf[i, 0:n] = lax.dot_general(keys, q_cat[q], (((1,), (1,)), ((), ())), preferred_element_type=F32)
        for i, q in enumerate(qs):
            scores = s_buf[i, 0:n]
            old_max = stats[q, 0:1, :]
            new_max = jnp.maximum(old_max, jnp.max(scores, axis=0, keepdims=True))
            r_buf[i, 0:1, :] = jnp.exp2(old_max - new_max)
            stats[q, 0:1, :] = new_max
            w_buf[i, 0:n] = jnp.exp2(scores - new_max).astype(BF16)
        for i, q in enumerate(qs):
            yield o_acc[q] * r_buf[i, 0:1, :] + jnp.dot(values, w_buf[i, 0:n], preferred_element_type=F32)

    def d_push(offset):
        slot = ring(qa, offset)
        push(o_send.at[slot], o_recv.at[qa], O, d_recv.at[0], q_dev(offset))
        push(stats.at[slot], st_recv.at[qa], ST, d_recv.at[1], q_dev(offset))

    def key_step(step, _):
        for s in (1, 2, 3):

            @pl.when(step == s)
            def _(s=s):
                kv_step(s, other_chunks if s == 1 else range(KV_CHUNKS))
                for d in (s, -s):
                    open_keys(ring(ka, d))

        ks = (lax.rem(ka + step, RING), lax.rem(ka - step + RING, RING))
        for q, out in enumerate(key_blocks(ks, range(8))):
            o_acc[q] = out
        return 0

    phase("k1")
    kv_step(1, first_chunks)
    phase("own_keys")
    for q, out in enumerate(key_blocks((ka,), range(8))):
        o_acc[q] = out
    phase("keys")
    lax.fori_loop(1, 4, key_step, 0)
    phase("k4")
    arrived(kv_all.at[0], kv_recv.at[3 * KV_CHUNKS])
    open_keys(ring(ka, 4))
    phase("last_keys")
    offsets = (4, 3, 5, 2, 6, 1, 7, 0)
    qs = [ring(qa, offset) for offset in offsets]
    for i, out in enumerate(key_blocks((ring(ka, 4),), qs)):
        stats[qs[i], 1:2, :] = out[128:129]
        if offsets[i]:
            o_send[qs[i]] = out[0:128].astype(BF16)
        else:
            o_acc[qa] = out
        if i in (2, 4, 6):
            for offset in offsets[0 if i == 2 else i - 1 : i + 1]:
                d_push(offset)
    phase("d_wait")
    arrived(st_recv.at[pl.ds(0, 7)], d_recv.at[1])
    arrived(o_recv.at[pl.ds(0, 7)], d_recv.at[0])
    phase("merge")
    whole_max = stats[qa, 0:1, :]
    for offset in range(1, 8):
        whole_max = jnp.maximum(whole_max, st_recv[ring(qa, offset), 0:1, :])
    weight = jnp.exp2(stats[qa, 0:1, :] - whole_max)
    whole_sum = stats[qa, 1:2, :] * weight
    whole_out = o_acc[qa, 0:128, :] * weight
    for offset in range(1, 8):
        slot = ring(qa, offset)
        weight = jnp.exp2(st_recv[slot, 0:1, :] - whole_max)
        whole_sum += st_recv[slot, 1:2, :] * weight
        whole_out += o_recv[slot].astype(F32) * weight
    lws_ref[...] = whole_max * (1.0 / LOG2E) + jnp.log(whole_sum)
    cat[:, 0:128] = jnp.transpose(whole_out / whole_sum).astype(BF16)

    phase("out_mate")
    def rows_of(xx, cc):
        return pl.ds(pl.multiple_of((2 * xx + cc) * 32, 32), 32)

    order = [chip(2), chip(1), chip(3), x]
    for_mate = jnp.concatenate([cat[rows_of(xx, 1 - c), :] for xx in order], axis=0)
    for n in range(4):
        cols = slice(512 * n, 512 * n + 512)
        part = jnp.dot(for_mate, wout[:, cols], preferred_element_type=F32).astype(BF16)
        for j in range(4):
            e_psend[j, :, cols] = part[32 * j : 32 * j + 32]
    for j in range(4):
        push(e_psend.at[j], e_precv.at[j], EP, ep_recv.at[j], mate)
    phase("out_own")
    for_own = jnp.concatenate([cat[rows_of(xx, c), :] for xx in order], axis=0)
    for n in range(4):
        cols = slice(512 * n, 512 * n + 512)
        part = jnp.dot(for_own, wout[:, cols], preferred_element_type=F32)
        for j in range(4):
            e_own[j, :, cols] = part[32 * j : 32 * j + 32]
    phase("e_mate")
    for j in range(3):
        arrived(e_precv.at[j], ep_recv.at[j])
        e_xsend[j] = (e_own[j] + e_precv[j].astype(F32)).astype(BF16)
        push(e_xsend.at[j], e_xrecv.at[j], EX, ex_recv.at[0], t_dev(order[j], c))
    phase("e_sum")
    arrived(e_precv.at[3], ep_recv.at[3])
    total = e_own[3] + e_precv[3].astype(F32)
    arrived(e_xrecv, ex_recv.at[0])
    for j in (1, 2, 0):
        total += e_xrecv[j].astype(F32)
    mixed_ref[...] = total.astype(BF16)
    phase("send_wait")
    for ref, send in (
        (act_all.at[pl.ds(0, 7)], A),
        (lat_all.at[pl.ds(0, 7)], L),
        (q_all.at[pl.ds(0, 7)], Q),
        (kv_all.at[pl.ds(0, 7)], KV),
        (o_send.at[pl.ds(0, 7)], O),
        (stats.at[pl.ds(0, 7)], ST),
        (e_psend, EP),
        (e_xsend, EX),
        (halo_out, H),
    ):
        remote(ref, ref, send, d_recv.at[0], mate).wait_send()
    phase(None)


def body(
    activations, norm_gain, query_weight, latent_weight, rope_key_weight, latent_gain, expand_weight,
    gate_weight, pre_weight, value_weight, conv_kernel, output_attend, output_conv,
):
    dma = pltpu.SemaphoreType.DMA
    vmem = pltpu.VMEM
    return pl.pallas_call(
        kernel,
        out_shape=(vmem((32, D), BF16), vmem((1, T), F32)),
        in_specs=[pl.BlockSpec(memory_space=pl.ANY)] * 14,
        out_specs=(pl.BlockSpec(memory_space=vmem), pl.BlockSpec(memory_space=vmem)),
        scratch_shapes=[
            vmem((8, T, 256), BF16),
            vmem((1, D), F32),
            vmem((1, 512), F32),
            vmem((512, 256), BF16),
            vmem((384, D), BF16),
            vmem((D, 384), BF16),
            vmem((3, 128), BF16),
            vmem((256, D), BF16),
            vmem((320, 256), F32),
            vmem((T, 384), F32),
            vmem((T, 384), F32),
            vmem((8, 128, 128), BF16),
            vmem((8, Q_ROWS, 128), BF16),
            vmem((8, T, 256), BF16),
            vmem((8, KV_ROWS, 128), BF16),
            vmem((8, T, 256), BF16),
            vmem((8, V_ROWS, T), BF16),
            vmem((8, 2 * T, T), F32),
            vmem((8, 2 * T, T), BF16),
            vmem((8, 8, T), F32),
            vmem((8, 8, T), F32),
            vmem((8, V_ROWS, T), F32),
            vmem((8, 128, T), BF16),
            vmem((8, 128, T), BF16),
            vmem((8, 8, T), F32),
            vmem((2, 8, 128), F32),
            vmem((2, 8, 128), F32),
            vmem((T, 256), BF16),
            vmem((4, 32, D), BF16),
            vmem((4, 32, D), BF16),
            vmem((4, 32, D), F32),
            vmem((3, 32, D), BF16),
            vmem((3, 32, D), BF16),
            dma((9,)),
            dma((9,)),
            dma((11,)),
            dma((4,)),
            dma((7,)),
            dma((3 * KV_CHUNKS + 1,)),
            dma((2,)),
            dma((1,)),
            dma((4,)),
            dma((1,)),
        ],
        compiler_params=pltpu.CompilerParams(collective_id=0, has_side_effects=True),
    )(
        activations, norm_gain.reshape(1, D), query_weight.T, latent_weight.T, rope_key_weight.T,
        latent_gain.reshape(1, 512), expand_weight, gate_weight, pre_weight, value_weight, conv_kernel,
        output_attend, output_conv, jnp.asarray(rotation_tables()),
    )


def solution(mesh):
    return jax.shard_map(
        body,
        mesh=mesh,
        in_specs=(
            P("sp", "tp"),
            P(),
            P(None, "tp"),
            P(None, "tp"),
            P(),
            P(),
            P(None, "tp"),
            P(None, "tp"),
            P(None, "tp"),
            P(None, "tp"),
            P(None, "tp"),
            P("tp", None),
            P("tp", None),
        ),
        out_specs=(P(("sp", "tp"), None), P("tp", "sp")),
        check_vma=False,
    )
```

time: 87.1 us -> 68.9 us (0.79); the launches traced: 86.9 us -> 67.8 us
  Pallas kernels: 78.8 us -> 65.9 us
  local copies, waits for them, and re-layouts: 7.42 us -> 1.22 us
    pallas_call x1, Pallas kernels: 78.8 us -> 65.9 us  [body(): pl.pallas_call(kernel, out_shape=(vmem((32, D), BF16), vmem((1, T), F32))...]
    unnamed x9 -> x2, local copies, waits for them, and re-layouts: 7.42 us -> 1.22 us
where the time goes in v2:
time: 68.9 us; the launch traced here: 67.8 us
  Pallas kernels  65.9 us (96%)
  local copies, waits for them, and re-layouts  1.22 us (2%)
    pallas_call x1, Pallas kernels, body(): pl.pallas_call(kernel, out_shape=(vmem((32, D), BF16), vmem((1, T), F32))...  65.9 us

profile of v2, /device:TPU:1, one launch (start us, length us, event | category | flops | bytes accessed | tf_op | source)
XLA Modules:
  0.0 67.8 jit_solution(11798105280510903062)
XLA Ops:
  0.6 65.9 %shard_map.149 = (bf16[32,2048]{1,0:T(8,128)(2,1)S(1)}, f32[1,256]{1,0:T(1,128)S(1)}) custom-call(bf16[256,256]{1,0:T(8,128)(2,1)} %act_hbm.1, f32[1,2048]{1,0:T(1,128)} %bitcast.8, bf16[192,2048]{1,0:T(8,128)(2,1)} %bitcast.5, bf16[64,2048]{1,0:T(8,128)(2,1)} %bitcast.6, bf16[64,2048]{1,0:T(8,128)(2,1)} %bitcast.7, f32[1,512]{1,0:T(1,128)} %bitcast.9, ...), custom_call_target="tpu_custom_call" | custom-call | tf_op jit(solution)/shard_map/pallas_call | solution.py:478
  66.6 0.7 copy.18
  67.2 0.6 copy.19

commit v3 on v2

--- a/solution.py
+++ b/solution.py
@@ -22,7 +22,7 @@
 NX = 4
 T = 256
 Q_ROWS = 384
-KV_ROWS, KV_CHUNKS = 640, 4
+KV_ROWS = 640
 V_ROWS = 144
 LOW = -3.0e38
 LOG2E = 1.4426950408889634
@@ -50,10 +50,10 @@
     act_hbm, gain_hbm, qw_hbm, lw_hbm, rw_hbm, lgain_hbm, ew_hbm, gw_hbm, pw_hbm, vw_hbm, ck_hbm, oa_hbm, oc_hbm,
     table_hbm,
     mixed_ref, lws_ref,
-    act_all, gain, lgain, ew, wt, wb, ck, wout, table, acc, acc_b, lat_all,
+    act_all, gain, lgain, ew, wt, wb, ck, wa_all, wc, table, acc, acc_b, lat_all,
     q_all, q_cat, kv_all, k_cat, vt_all, s_buf, w_buf, r_buf, stats, o_acc, o_send, o_recv, st_recv,
-    halo_out, halo_in, cat, e_psend, e_precv, e_own, e_xsend, e_xrecv,
-    load_sem, sent, a_recv, l_recv, q_recv, kv_recv, d_recv, h_recv, ep_recv, ex_recv,
+    halo_out, halo_in, conv_mixed, attended, heads, e_psend, e_precv, e_own, e_xsend, e_xrecv,
+    load_sem, sent, a_recv, l_recv, q_recv, kv_recv, d_recv, h_recv, ep_recv, ex_recv, w_recv, at_recv,
 ):
     sp = lax.axis_index("sp")
     tp = lax.axis_index("tp")
@@ -78,7 +78,7 @@
         return (sp, 2 * xx + cc)
 
     scopes = []
-    A, L, Q, KV, O, ST, EP, EX, H = (sent.at[i] for i in range(9))
+    A, L, Q, KV, O, ST, EP, EX, H, W, AT = (sent.at[i] for i in range(11))
 
     def phase(name):
         if scopes:
@@ -125,12 +125,13 @@
     load(5, (table_hbm, table))
     load(6, (ck_hbm, ck))
     load(7, (ew_hbm, ew))
-    load(8, (oa_hbm, wout.at[pl.ds(0, 128), :]), (oc_hbm, wout.at[pl.ds(128, 128), :]))
+    load(8, (oa_hbm, wa_all.at[tp]))
+    load(9, (oc_hbm, wc))
 
     phase("barrier")
     barrier = pltpu.get_barrier_semaphore()
     partners = [(sp, lax.rem(tp + k, 8)) for k in range(1, 8)]
-    partners += [q_dev(k) for k in range(1, 8)] + [k_dev(1), k_dev(-1)]
+    partners += [q_dev(k) for k in range(1, 8)] + [k_dev(k) for k in (1, -1, 2, -2)]
     after, before = (lax.rem(sp + 1, 64), tp), (lax.rem(sp + 63, 64), tp)
     partners += [after, before]
     for dev in partners:
@@ -215,7 +216,8 @@
     loaded(5, table)
     loaded(6, ck)
     loaded(7, ew)
-    loaded(8, wout)
+    loaded(8, wa_all.at[tp])
+    loaded(9, wc)
     scale = (NOPE + ROPE) ** (-0.5) * LOG2E
     q_all[qa, 0:256, :] = (acc[:, 0:128] * inv_rms * scale).astype(BF16)
     raw = acc[:, 128:256] * inv_rms
@@ -227,34 +229,49 @@
     swapped = pltpu.roll(rotated, 64, 1)
     q_all[qa, 256:384, :] = (jnp.where(low, rotated[0:128], swapped[128:256]) * scale).astype(BF16)
 
-    def q_push(offset, ch, n, recv, to):
-        part = q_all.at[ring(qa, offset), pl.ds(192 * ch, 192 * n), :]
-        push(part, part, Q, q_recv.at[recv], q_dev(to))
-
-    def q_wait(n, recv):
-        arrived(q_all.at[pl.ds(0, n)] if n else q_all.at[0, pl.ds(0, 192), :], q_recv.at[recv])
-
-    q_push(0, 0, 2, 0, 1)
-    q_push(0, 0, 2, 1, -1)
-    q_push(0, 0, 1, 2, 2)
-    q_push(0, 1, 1, 3, -2)
-    q_push(0, 1, 1, 4, 2)
-    q_push(0, 0, 1, 4, -2)
-
-    n_kv = KV_ROWS // KV_CHUNKS
-
-    def kv_push(step, ch, to):
-        part = kv_all.at[ring(ka, -to * step), pl.ds(ch * n_kv, n_kv), :]
-        recv = step * KV_CHUNKS + ch if step < 3 else 3 * KV_CHUNKS
-        push(part, part, KV, kv_recv.at[recv], k_dev(to))
-
-    def kv_step(step, some):
-        for ch in some:
-            arrived(kv_all.at[0, pl.ds(0, 2 * n_kv), :], kv_recv.at[(step - 1) * KV_CHUNKS + ch])
-            if step < 3 or ch < KV_CHUNKS // 2:
-                kv_push(step, ch, 1)
-            if step < 3 or ch >= KV_CHUNKS // 2:
-                kv_push(step, ch, -1)
+    def spread(blocks, pos, rows, lead, stage, recv, dev):
+        def move(offset, row, n, sem, to):
+            part = blocks.at[ring(pos, offset), pl.ds(row, n), :]
+            push(part, part, stage, recv.at[sem], dev(to))
+
+        half, n = rows // 2, rows // 2 // lead
+
+        def begin():
+            for i in range(lead):
+                move(0, i * n, n, i, 2)
+                move(0, half + i * n, n, i, -2)
+            move(0, 0, rows, lead + 1, 1)
+            move(0, 0, rows, lead + 1, -1)
+            move(0, half, half, lead, 2)
+            move(0, 0, half, lead, -2)
+
+        def onward_lead():
+            for i in range(lead):
+                arrived(blocks.at[0, pl.ds(0, 2 * n), :], recv.at[i])
+                move(-2, i * n, n, lead + 3, 2)
+                move(2, half + i * n, n, lead + 3, -2)
+                move(-2, i * n, n, lead + 2, 1)
+                move(2, half + i * n, n, lead + 2, -1)
+
+        def onward_rest():
+            arrived(blocks.at[0], recv.at[lead])
+            move(-2, half, half, lead + 2, 1)
+            move(2, 0, half, lead + 2, -1)
+
+        def near():
+            arrived(blocks.at[pl.ds(0, 2)], recv.at[lead + 1])
+
+        def third():
+            arrived(blocks.at[pl.ds(0, 2)], recv.at[lead + 2])
+
+        def fourth():
+            arrived(blocks.at[0], recv.at[lead + 3])
+
+        return begin, onward_lead, onward_rest, near, third, fourth
+
+    q_begin, q_onward_lead, q_onward_rest, q_near, q_third, q_fourth = spread(q_all, qa, Q_ROWS, 1, Q, q_recv, q_dev)
+    k_begin, k_onward_lead, k_onward_rest, k_near, k_third, k_fourth = spread(kv_all, ka, KV_ROWS, 2, KV, kv_recv, k_dev)
+    q_begin()
 
     def open_query(slot):
         paired = q_all[slot, 256:384, :].astype(F32)
@@ -279,6 +296,32 @@
     gate = acc_b[:, 0:128] * inv_rms
 
     phase("latent_wait")
+    def w_push(slot, h, n, recv, dev):
+        part = wa_all.at[slot, pl.ds(64 * h, 64 * n), :]
+        push(part, part, W, w_recv.at[recv], dev)
+
+    def w_start():
+        w_push(tp, 0, 1, 0, up)
+        w_push(tp, 1, 1, 1, down)
+        w_push(tp, 0, 2, 4, mate)
+        w_push(tp, 1, 1, 2, up)
+        w_push(tp, 0, 1, 2, down)
+
+    def w_onward():
+        arrived(wa_all.at[0, pl.ds(0, 64), :], w_recv.at[0])
+        w_push(s_down, 0, 1, 3, up)
+        arrived(wa_all.at[0, pl.ds(0, 64), :], w_recv.at[1])
+        w_push(s_up, 1, 1, 3, down)
+
+    def w_near_to_mate():
+        arrived(wa_all.at[0], w_recv.at[2])
+        w_push(s_down, 0, 2, 4, mate)
+        w_push(s_up, 0, 2, 4, mate)
+
+    def w_far_to_mate():
+        arrived(wa_all.at[0], w_recv.at[3])
+        w_push(s_far, 0, 2, 4, mate)
+
     kv_rope = jnp.where(low, swapped[0:128], rotated[128:256]).astype(BF16)
     kv_all[ka, 256:384, :] = kv_rope
     open_query(qa)
@@ -287,20 +330,13 @@
     o_acc[...] = jnp.zeros_like(o_acc)
     ones = lax.broadcasted_iota(jnp.int32, (8, V_ROWS - 128, T), 1) == 0
     vt_all[:, 128:V_ROWS, :] = jnp.where(ones, 1.0, 0.0).astype(BF16)
-    phase("q1")
-    q_wait(1, 0)
-    q_push(-1, 0, 2, 5, 2)
-    q_wait(1, 1)
-    q_push(1, 0, 2, 5, -2)
     phase("latent_x")
     for recv, slot in ((1, s_down), (2, s_up), (0, s_far)):
         arrived(lat_all.at[0], l_recv.at[recv])
         l_push(slot, 3, mate)
     phase("q2")
-    q_wait(0, 2)
-    q_push(-2, 0, 1, 6, 2)
-    q_wait(0, 3)
-    q_push(2, 1, 1, 6, -2)
+    q_onward_lead()
+    w_start()
     phase("latent_mate")
     arrived(lat_all.at[pl.ds(0, 4)], l_recv.at[3])
 
@@ -317,10 +353,9 @@
     expanded = jnp.dot(latent, ew[...], preferred_element_type=F32).astype(BF16)
     kv_all[ka, 0:256, :] = expanded[:, 0:128]
     kv_all[ka, 384:640, :] = expanded[:, 128:256]
-    for ch in range(KV_CHUNKS):
-        kv_push(0, ch, 1)
-        kv_push(0, ch, -1)
-
+    k_begin()
+    phase("q2_rest")
+    q_onward_rest()
     phase("conv")
     arrived(halo_in, h_recv.at[0])
     row = lax.broadcasted_iota(jnp.int32, (T, 128), 0)
@@ -330,21 +365,29 @@
     shifted_up = jnp.where(row == T - 1, last, pltpu.roll(pre_mix, T - 1, 0))
     taps = ck[...].astype(F32)
     convolved = taps[0:1] * shifted_down + taps[1:2] * pre_mix + taps[2:3] * shifted_up
-    cat[:, 128:256] = (gate * convolved).astype(BF16)
+    conv_mixed[...] = (gate * convolved).astype(BF16)
     open_keys(ka)
 
-    phase("q_rest")
-    first_chunks, other_chunks = range(KV_CHUNKS // 2), range(KV_CHUNKS // 2, KV_CHUNKS)
-    q_wait(1, 4)
-    for offset in (1, -1, 2, -2):
-        open_query(ring(qa, offset))
-    phase("q3")
-    q_wait(2, 5)
-    for offset in (3, -3):
-        open_query(ring(qa, offset))
-    phase("q4")
-    q_wait(1, 6)
-    open_query(ring(qa, 4))
+    phase("conv_out")
+
+    def rows_of(xx, cc):
+        return pl.ds(pl.multiple_of((2 * xx + cc) * 32, 32), 32)
+
+    order = [chip(2), chip(1), chip(3), x]
+    for_mate = jnp.concatenate([conv_mixed[rows_of(xx, 1 - c), :] for xx in order], axis=0)
+    for n in range(4):
+        cols = slice(512 * n, 512 * n + 512)
+        part = jnp.dot(for_mate, wc[:, cols], preferred_element_type=F32).astype(BF16)
+        for j in range(4):
+            e_psend[j, :, cols] = part[32 * j : 32 * j + 32]
+    for j in range(4):
+        push(e_psend.at[j], e_precv.at[j], EP, ep_recv.at[j], mate)
+    for_own = jnp.concatenate([conv_mixed[rows_of(xx, c), :] for xx in order], axis=0)
+    for n in range(4):
+        cols = slice(512 * n, 512 * n + 512)
+        part = jnp.dot(for_own, wc[:, cols], preferred_element_type=F32)
+        for j in range(4):
+            e_own[j, :, cols] = part[32 * j : 32 * j + 32]
 
     def key_blocks(ks, qs):
         n = len(ks) * T
@@ -362,47 +405,90 @@
         for i, q in enumerate(qs):
             yield o_acc[q] * r_buf[i, 0:1, :] + jnp.dot(values, w_buf[i, 0:n], preferred_element_type=F32)
 
+    def attend(ks, qs):
+        for q, out in zip(qs, key_blocks(ks, qs)):
+            o_acc[q] = out
+
     def d_push(offset):
         slot = ring(qa, offset)
         push(o_send.at[slot], o_recv.at[qa], O, d_recv.at[0], q_dev(offset))
         push(stats.at[slot], st_recv.at[qa], ST, d_recv.at[1], q_dev(offset))
 
     def key_step(step, _):
-        for s in (1, 2, 3):
+        for s in (1, 2):
 
             @pl.when(step == s)
             def _(s=s):
-                kv_step(s, other_chunks if s == 1 else range(KV_CHUNKS))
+                if s == 1:
+                    k_near()
+                if s == 2:
+                    k_onward_rest()
+                    w_onward()
+                    conv_onward()
                 for d in (s, -s):
                     open_keys(ring(ka, d))
 
         ks = (lax.rem(ka + step, RING), lax.rem(ka - step + RING, RING))
-        for q, out in enumerate(key_blocks(ks, range(8))):
-            o_acc[q] = out
+        attend(ks, range(8))
         return 0
 
-    phase("k1")
-    kv_step(1, first_chunks)
+    def conv_onward():
+        for j in range(3):
+            push(e_xsend.at[j], e_xrecv.at[j], EX, ex_recv.at[0], t_dev(order[j], c))
+
+    phase("q_rest")
+    q_near()
+    for offset in (1, -1, 2, -2):
+        open_query(ring(qa, offset))
+    own = (ka,)
     phase("own_keys")
-    for q, out in enumerate(key_blocks((ka,), range(8))):
-        o_acc[q] = out
+    attend(own, [ring(qa, offset) for offset in (0, 1, -1, 2, -2)])
+    phase("k_lead")
+    k_onward_lead()
+    phase("q3")
+    q_third()
+    for offset in (3, -3):
+        open_query(ring(qa, offset))
+    phase("q4")
+    q_fourth()
+    open_query(ring(qa, 4))
+
+    phase("own_rest")
+    attend(own, [ring(qa, offset) for offset in (3, -3, 4)])
+    phase("conv_mate")
+    for j in range(4):
+        arrived(e_precv.at[j], ep_recv.at[j])
+        both = e_own[j] + e_precv[j].astype(F32)
+        if j < 3:
+            e_xsend[j] = both.astype(BF16)
+        else:
+            e_own[j] = both
     phase("keys")
-    lax.fori_loop(1, 4, key_step, 0)
+    lax.fori_loop(1, 3, key_step, 0)
     phase("k4")
-    arrived(kv_all.at[0], kv_recv.at[3 * KV_CHUNKS])
+    k_fourth()
     open_keys(ring(ka, 4))
+    attend((ring(ka, 4),), range(8))
+    phase("k3")
+    k_third()
+    for d in (3, -3):
+        open_keys(ring(ka, d))
     phase("last_keys")
-    offsets = (4, 3, 5, 2, 6, 1, 7, 0)
-    qs = [ring(qa, offset) for offset in offsets]
-    for i, out in enumerate(key_blocks((ring(ka, 4),), qs)):
-        stats[qs[i], 1:2, :] = out[128:129]
-        if offsets[i]:
-            o_send[qs[i]] = out[0:128].astype(BF16)
-        else:
-            o_acc[qa] = out
-        if i in (2, 4, 6):
-            for offset in offsets[0 if i == 2 else i - 1 : i + 1]:
+    for offsets in ((4, 3, 5), (2, 6), (1, 7, 0)):
+        qs = [ring(qa, offset) for offset in offsets]
+        for offset, q, out in zip(offsets, qs, key_blocks((ring(ka, 3), ring(ka, -3)), qs)):
+            stats[q, 1:2, :] = out[128:129]
+            if offset:
+                o_send[q] = out[0:128].astype(BF16)
+            else:
+                o_acc[qa] = out
+        for offset in offsets:
+            if offset:
                 d_push(offset)
+    phase("w_near")
+    w_near_to_mate()
+    phase("w_far")
+    w_far_to_mate()
     phase("d_wait")
     arrived(st_recv.at[pl.ds(0, 7)], d_recv.at[1])
     arrived(o_recv.at[pl.ds(0, 7)], d_recv.at[0])
@@ -419,40 +505,28 @@
         whole_sum += st_recv[slot, 1:2, :] * weight
         whole_out += o_recv[slot].astype(F32) * weight
     lws_ref[...] = whole_max * (1.0 / LOG2E) + jnp.log(whole_sum)
-    cat[:, 0:128] = jnp.transpose(whole_out / whole_sum).astype(BF16)
-
-    phase("out_mate")
-    def rows_of(xx, cc):
-        return pl.ds(pl.multiple_of((2 * xx + cc) * 32, 32), 32)
-
-    order = [chip(2), chip(1), chip(3), x]
-    for_mate = jnp.concatenate([cat[rows_of(xx, 1 - c), :] for xx in order], axis=0)
+    attended[...] = jnp.transpose(whole_out / whole_sum).astype(BF16)
+
+    phase("heads")
+    for k in range(1, 8):
+        peer = lax.rem(tp + k, 8)
+        rows = pl.ds(pl.multiple_of(peer * 32, 32), 32)
+        push(attended.at[rows, :], heads.at[tp], AT, at_recv.at[0], (sp, peer))
+    heads[tp] = attended[pl.ds(pl.multiple_of(tp * 32, 32), 32), :]
+    phase("conv_sum")
+    arrived(e_xrecv, ex_recv.at[0])
+    e_own[3] = e_own[3] + e_xrecv[0].astype(F32) + e_xrecv[1].astype(F32) + e_xrecv[2].astype(F32)
+    phase("w_wait")
+    arrived(wa_all.at[pl.ds(0, 4)], w_recv.at[4])
+    phase("heads_wait")
+    arrived(heads.at[pl.ds(0, 7)], at_recv.at[0])
+    phase("out")
+    side_by_side = jnp.concatenate([heads[j] for j in range(8)], axis=1)
     for n in range(4):
         cols = slice(512 * n, 512 * n + 512)
-        part = jnp.dot(for_mate, wout[:, cols], preferred_element_type=F32).astype(BF16)
-        for j in range(4):
-            e_psend[j, :, cols] = part[32 * j : 32 * j + 32]
-    for j in range(4):
-        push(e_psend.at[j], e_precv.at[j], EP, ep_recv.at[j], mate)
-    phase("out_own")
-    for_own = jnp.concatenate([cat[rows_of(xx, c), :] for xx in order], axis=0)
-    for n in range(4):
-        cols = slice(512 * n, 512 * n + 512)
-        part = jnp.dot(for_own, wout[:, cols], preferred_element_type=F32)
-        for j in range(4):
-            e_own[j, :, cols] = part[32 * j : 32 * j + 32]
-    phase("e_mate")
-    for j in range(3):
-        arrived(e_precv.at[j], ep_recv.at[j])
-        e_xsend[j] = (e_own[j] + e_precv[j].astype(F32)).astype(BF16)
-        push(e_xsend.at[j], e_xrecv.at[j], EX, ex_recv.at[0], t_dev(order[j], c))
-    phase("e_sum")
-    arrived(e_precv.at[3], ep_recv.at[3])
-    total = e_own[3] + e_precv[3].astype(F32)
-    arrived(e_xrecv, ex_recv.at[0])
-    for j in (1, 2, 0):
-        total += e_xrecv[j].astype(F32)
-    mixed_ref[...] = total.astype(BF16)
+        weights = wa_all[:, :, cols].reshape(1024, 512)
+        out = jnp.dot(side_by_side, weights, preferred_element_type=F32)
+        mixed_ref[:, cols] = (out + e_own[3, :, cols]).astype(BF16)
     phase("send_wait")
     for ref, send in (
         (act_all.at[pl.ds(0, 7)], A),
@@ -464,6 +538,8 @@
         (e_psend, EP),
         (e_xsend, EX),
         (halo_out, H),
+        (wa_all.at[pl.ds(0, 7)], W),
+        (heads.at[pl.ds(0, 7)], AT),
     ):
         remote(ref, ref, send, d_recv.at[0], mate).wait_send()
     phase(None)
@@ -488,7 +564,8 @@
             vmem((384, D), BF16),
             vmem((D, 384), BF16),
             vmem((3, 128), BF16),
-            vmem((256, D), BF16),
+            vmem((8, 128, D), BF16),
+            vmem((128, D), BF16),
             vmem((320, 256), F32),
             vmem((T, 384), F32),
             vmem((T, 384), F32),
@@ -508,21 +585,25 @@
             vmem((8, 8, T), F32),
             vmem((2, 8, 128), F32),
             vmem((2, 8, 128), F32),
-            vmem((T, 256), BF16),
+            vmem((T, 128), BF16),
+            vmem((T, 128), BF16),
+            vmem((8, 32, 128), BF16),
             vmem((4, 32, D), BF16),
             vmem((4, 32, D), BF16),
             vmem((4, 32, D), F32),
             vmem((3, 32, D), BF16),
             vmem((3, 32, D), BF16),
-            dma((9,)),
-            dma((9,)),
+            dma((10,)),
+            dma((11,)),
             dma((11,)),
             dma((4,)),
-            dma((7,)),
-            dma((3 * KV_CHUNKS + 1,)),
+            dma((5,)),
+            dma((6,)),
             dma((2,)),
             dma((1,)),
             dma((4,)),
+            dma((1,)),
+            dma((5,)),
             dma((1,)),
         ],
         compiler_params=pltpu.CompilerParams(collective_id=0, has_side_effects=True),

time: 68.9 us -> 59.7 us (0.87); the launches traced: 67.8 us -> 59.5 us
  Pallas kernels: 65.9 us -> 57.7 us
    pallas_call x1, Pallas kernels: 65.9 us -> 57.7 us  [body(): pl.pallas_call(kernel, out_shape=(vmem((32, D), BF16), vmem((1, T), F32))...]
where the time goes in v3:
time: 59.7 us; the launch traced here: 59.5 us
  Pallas kernels  57.7 us (97%)
  local copies, waits for them, and re-layouts  1.22 us (2%)
  between operations  0.64 us (1%)
    pallas_call x1, Pallas kernels, body(): pl.pallas_call(kernel, out_shape=(vmem((32, D), BF16), vmem((1, T), F32))...  57.7 us
    unnamed x2, local copies, waits for them, and re-layouts  1.22 us

profile of v3, /device:TPU:1, one launch (start us, length us, event | category | flops | bytes accessed | tf_op | source)
XLA Modules:
  0.0 59.5 jit_solution(6624753022196209048)
XLA Ops:
  0.6 57.7 %shard_map.149 = (bf16[32,2048]{1,0:T(8,128)(2,1)S(1)}, f32[1,256]{1,0:T(1,128)S(1)}) custom-call(bf16[256,256]{1,0:T(8,128)(2,1)} %act_hbm.1, f32[1,2048]{1,0:T(1,128)} %bitcast.8, bf16[192,2048]{1,0:T(8,128)(2,1)} %bitcast.5, bf16[64,2048]{1,0:T(8,128)(2,1)} %bitcast.6, bf16[64,2048]{1,0:T(8,128)(2,1)} %bitcast.7, f32[1,512]{1,0:T(1,128)} %bitcast.9, ...), custom_call_target="tpu_custom_call" | custom-call | tf_op jit(solution)/shard_map/pallas_call | solution.py:554
  58.3 0.7 %copy.18 = bf16[32,2048]{1,0:T(8,128)(2,1)} copy(bf16[32,2048]{1,0:T(8,128)(2,1)S(1)} %get-tuple-element.2) | data formatting | bytes 262144
  59.0 0.6 copy.19

commit v4 on v3

--- a/solution.py
+++ b/solution.py
@@ -22,7 +22,7 @@
 NX = 4
 T = 256
 Q_ROWS = 384
-KV_ROWS = 640
+KV_ROWS, ROPE_ROWS = 512, 128
 V_ROWS = 144
 LOW = -3.0e38
 LOG2E = 1.4426950408889634
@@ -51,9 +51,9 @@
     table_hbm,
     mixed_ref, lws_ref,
     act_all, gain, lgain, ew, wt, wb, ck, wa_all, wc, table, acc, acc_b, lat_all,
-    q_all, q_cat, kv_all, k_cat, vt_all, s_buf, w_buf, r_buf, stats, o_acc, o_send, o_recv, st_recv,
+    q_all, q_cat, kv_all, rope_all, k_cat, vt_all, s_buf, w_buf, r_buf, stats, o_acc, o_send, o_recv, st_recv,
     halo_out, halo_in, conv_mixed, attended, heads, e_psend, e_precv, e_own, e_xsend, e_xrecv,
-    load_sem, sent, a_recv, l_recv, q_recv, kv_recv, d_recv, h_recv, ep_recv, ex_recv, w_recv, at_recv,
+    load_sem, sent, a_recv, l_recv, q_recv, kv_recv, r_recv, d_recv, h_recv, ep_recv, ex_recv, w_recv, at_recv,
 ):
     sp = lax.axis_index("sp")
     tp = lax.axis_index("tp")
@@ -78,7 +78,7 @@
         return (sp, 2 * xx + cc)
 
     scopes = []
-    A, L, Q, KV, O, ST, EP, EX, H, W, AT = (sent.at[i] for i in range(11))
+    A, L, Q, KV, O, ST, EP, EX, H, W, AT, R = (sent.at[i] for i in range(12))
 
     def phase(name):
         if scopes:
@@ -131,7 +131,7 @@
     phase("barrier")
     barrier = pltpu.get_barrier_semaphore()
     partners = [(sp, lax.rem(tp + k, 8)) for k in range(1, 8)]
-    partners += [q_dev(k) for k in range(1, 8)] + [k_dev(k) for k in (1, -1, 2, -2)]
+    partners += [dev(k) for dev in (q_dev, k_dev) for k in (1, -1, 2, -2)]
     after, before = (lax.rem(sp + 1, 64), tp), (lax.rem(sp + 63, 64), tp)
     partners += [after, before]
     for dev in partners:
@@ -201,6 +201,32 @@
     phase("latent_send")
     inv_rms = lax.rsqrt(jnp.sum(squares, axis=1, keepdims=True) / D + EPSILON)
 
+    def w_push(slot, h, n, recv, dev):
+        part = wa_all.at[slot, pl.ds(64 * h, 64 * n), :]
+        push(part, part, W, w_recv.at[recv], dev)
+
+    def w_start():
+        w_push(tp, 0, 1, 0, up)
+        w_push(tp, 1, 1, 1, down)
+        w_push(tp, 0, 2, 4, mate)
+        w_push(tp, 1, 1, 2, up)
+        w_push(tp, 0, 1, 2, down)
+
+    def w_onward():
+        arrived(wa_all.at[0, pl.ds(0, 64), :], w_recv.at[0])
+        w_push(s_down, 0, 1, 3, up)
+        arrived(wa_all.at[0, pl.ds(0, 64), :], w_recv.at[1])
+        w_push(s_up, 1, 1, 3, down)
+
+    def w_near_to_mate():
+        arrived(wa_all.at[0], w_recv.at[2])
+        w_push(s_down, 0, 2, 4, mate)
+        w_push(s_up, 0, 2, 4, mate)
+
+    def w_far_to_mate():
+        arrived(wa_all.at[0], w_recv.at[3])
+        w_push(s_far, 0, 2, 4, mate)
+
     low = lane_iota(128) < 64
     latent_part = acc[:, 256:384] * inv_rms
     lat_all[tp] = jnp.where(low, latent_part[0:128], latent_part[128:256]).astype(BF16)
@@ -210,13 +236,14 @@
 
     for i, dev in enumerate((t_dev(chip(2), c), up, down, mate)):
         l_push(tp, i, dev)
+    loaded(8, wa_all.at[tp])
+    w_start()
 
     phase("query")
     loaded(4, lgain)
     loaded(5, table)
     loaded(6, ck)
     loaded(7, ew)
-    loaded(8, wa_all.at[tp])
     loaded(9, wc)
     scale = (NOPE + ROPE) ** (-0.5) * LOG2E
     q_all[qa, 0:256, :] = (acc[:, 0:128] * inv_rms * scale).astype(BF16)
@@ -270,8 +297,10 @@
         return begin, onward_lead, onward_rest, near, third, fourth
 
     q_begin, q_onward_lead, q_onward_rest, q_near, q_third, q_fourth = spread(q_all, qa, Q_ROWS, 1, Q, q_recv, q_dev)
+    r_begin, r_onward_lead, r_onward_rest, r_near, r_third, r_fourth = spread(rope_all, ka, ROPE_ROWS, 1, R, r_recv, k_dev)
     k_begin, k_onward_lead, k_onward_rest, k_near, k_third, k_fourth = spread(kv_all, ka, KV_ROWS, 2, KV, kv_recv, k_dev)
     q_begin()
+    rope_all[ka] = jnp.where(low, swapped[0:128], rotated[128:256]).astype(BF16)
 
     def open_query(slot):
         paired = q_all[slot, 256:384, :].astype(F32)
@@ -280,11 +309,11 @@
         q_cat[slot, 128:256, 128:256] = jnp.where(low, pltpu.roll(paired, 64, 1), 0.0).astype(BF16)
 
     def open_keys(slot):
-        paired = kv_all[slot, 256:384, :]
+        paired = rope_all[slot]
         k_cat[slot, :, 0:128] = kv_all[slot, 0:256, :]
         k_cat[slot, 0:128, 128:256] = paired
         k_cat[slot, 128:256, 128:256] = pltpu.roll(paired.astype(F32), 64, 1).astype(BF16)
-        vt_all[slot, 0:128, :] = jnp.transpose(kv_all[slot, 384:640, :].astype(F32)).astype(BF16)
+        vt_all[slot, 0:128, :] = jnp.transpose(kv_all[slot, 256:512, :].astype(F32)).astype(BF16)
 
     phase("halo")
     pre_mix = (acc_b[:, 128:256] * inv_rms) * (acc_b[:, 256:384] * inv_rms)
@@ -296,34 +325,6 @@
     gate = acc_b[:, 0:128] * inv_rms
 
     phase("latent_wait")
-    def w_push(slot, h, n, recv, dev):
-        part = wa_all.at[slot, pl.ds(64 * h, 64 * n), :]
-        push(part, part, W, w_recv.at[recv], dev)
-
-    def w_start():
-        w_push(tp, 0, 1, 0, up)
-        w_push(tp, 1, 1, 1, down)
-        w_push(tp, 0, 2, 4, mate)
-        w_push(tp, 1, 1, 2, up)
-        w_push(tp, 0, 1, 2, down)
-
-    def w_onward():
-        arrived(wa_all.at[0, pl.ds(0, 64), :], w_recv.at[0])
-        w_push(s_down, 0, 1, 3, up)
-        arrived(wa_all.at[0, pl.ds(0, 64), :], w_recv.at[1])
-        w_push(s_up, 1, 1, 3, down)
-
-    def w_near_to_mate():
-        arrived(wa_all.at[0], w_recv.at[2])
-        w_push(s_down, 0, 2, 4, mate)
-        w_push(s_up, 0, 2, 4, mate)
-
-    def w_far_to_mate():
-        arrived(wa_all.at[0], w_recv.at[3])
-        w_push(s_far, 0, 2, 4, mate)
-
-    kv_rope = jnp.where(low, swapped[0:128], rotated[128:256]).astype(BF16)
-    kv_all[ka, 256:384, :] = kv_rope
     open_query(qa)
     stats[:, 0:1, :] = jnp.full((8, 1, T), LOW, F32)
     stats[:, 1:8, :] = jnp.zeros((8, 7, T), F32)
@@ -334,9 +335,9 @@
     for recv, slot in ((1, s_down), (2, s_up), (0, s_far)):
         arrived(lat_all.at[0], l_recv.at[recv])
         l_push(slot, 3, mate)
+    r_begin()
     phase("q2")
     q_onward_lead()
-    w_start()
     phase("latent_mate")
     arrived(lat_all.at[pl.ds(0, 4)], l_recv.at[3])
 
@@ -352,7 +353,7 @@
     latent = (parts * latent_inv * lgain[...]).astype(BF16)
     expanded = jnp.dot(latent, ew[...], preferred_element_type=F32).astype(BF16)
     kv_all[ka, 0:256, :] = expanded[:, 0:128]
-    kv_all[ka, 384:640, :] = expanded[:, 128:256]
+    kv_all[ka, 256:512, :] = expanded[:, 128:256]
     k_begin()
     phase("q2_rest")
     q_onward_rest()
@@ -420,11 +421,10 @@
             @pl.when(step == s)
             def _(s=s):
                 if s == 1:
+                    r_near()
                     k_near()
                 if s == 2:
                     k_onward_rest()
-                    w_onward()
-                    conv_onward()
                 for d in (s, -s):
                     open_keys(ring(ka, d))
 
@@ -443,6 +443,9 @@
     own = (ka,)
     phase("own_keys")
     attend(own, [ring(qa, offset) for offset in (0, 1, -1, 2, -2)])
+    phase("rope_onward")
+    r_onward_lead()
+    r_onward_rest()
     phase("k_lead")
     k_onward_lead()
     phase("q3")
@@ -453,6 +456,8 @@
     q_fourth()
     open_query(ring(qa, 4))
 
+    phase("w_onward")
+    w_onward()
     phase("own_rest")
     attend(own, [ring(qa, offset) for offset in (3, -3, 4)])
     phase("conv_mate")
@@ -463,13 +468,16 @@
             e_xsend[j] = both.astype(BF16)
         else:
             e_own[j] = both
+    conv_onward()
     phase("keys")
     lax.fori_loop(1, 3, key_step, 0)
     phase("k4")
+    r_fourth()
     k_fourth()
     open_keys(ring(ka, 4))
     attend((ring(ka, 4),), range(8))
     phase("k3")
+    r_third()
     k_third()
     for d in (3, -3):
         open_keys(ring(ka, d))
@@ -508,10 +516,10 @@
     attended[...] = jnp.transpose(whole_out / whole_sum).astype(BF16)
 
     phase("heads")
-    for k in range(1, 8):
-        peer = lax.rem(tp + k, 8)
+    for far, xx, cc in ((1, 2, c), (1, 2, 1 - c), (0, 1, c), (0, 1, 1 - c), (0, 3, c), (0, 3, 1 - c), (0, 0, 1 - c)):
+        peer = 2 * chip(xx) + cc
         rows = pl.ds(pl.multiple_of(peer * 32, 32), 32)
-        push(attended.at[rows, :], heads.at[tp], AT, at_recv.at[0], (sp, peer))
+        push(attended.at[rows, :], heads.at[tp], AT, at_recv.at[far], (sp, peer))
     heads[tp] = attended[pl.ds(pl.multiple_of(tp * 32, 32), 32), :]
     phase("conv_sum")
     arrived(e_xrecv, ex_recv.at[0])
@@ -519,13 +527,27 @@
     phase("w_wait")
     arrived(wa_all.at[pl.ds(0, 4)], w_recv.at[4])
     phase("heads_wait")
-    arrived(heads.at[pl.ds(0, 7)], at_recv.at[0])
+    arrived(heads.at[pl.ds(0, 5)], at_recv.at[0])
     phase("out")
-    side_by_side = jnp.concatenate([heads[j] for j in range(8)], axis=1)
+
+    def heads_of(xx):
+        slot = 2 * chip(xx)
+        return jnp.concatenate([heads[slot], heads[slot + 1]], axis=1), slot
+
+    near_heads = [heads_of(xx) for xx in (0, 1, 3)]
     for n in range(4):
         cols = slice(512 * n, 512 * n + 512)
-        weights = wa_all[:, :, cols].reshape(1024, 512)
-        out = jnp.dot(side_by_side, weights, preferred_element_type=F32)
+        out = e_own[3, :, cols]
+        for both, slot in near_heads:
+            out += jnp.dot(both, wa_all[pl.ds(slot, 2), :, cols].reshape(256, 512), preferred_element_type=F32)
+        e_own[3, :, cols] = out
+    phase("far_wait")
+    arrived(heads.at[pl.ds(0, 2)], at_recv.at[1])
+    phase("far_out")
+    both, slot = heads_of(2)
+    for n in range(4):
+        cols = slice(512 * n, 512 * n + 512)
+        out = jnp.dot(both, wa_all[pl.ds(slot, 2), :, cols].reshape(256, 512), preferred_element_type=F32)
         mixed_ref[:, cols] = (out + e_own[3, :, cols]).astype(BF16)
     phase("send_wait")
     for ref, send in (
@@ -533,6 +555,7 @@
         (lat_all.at[pl.ds(0, 7)], L),
         (q_all.at[pl.ds(0, 7)], Q),
         (kv_all.at[pl.ds(0, 7)], KV),
+        (rope_all.at[pl.ds(0, 7)], R),
         (o_send.at[pl.ds(0, 7)], O),
         (stats.at[pl.ds(0, 7)], ST),
         (e_psend, EP),
@@ -573,6 +596,7 @@
             vmem((8, Q_ROWS, 128), BF16),
             vmem((8, T, 256), BF16),
             vmem((8, KV_ROWS, 128), BF16),
+            vmem((8, ROPE_ROWS, 128), BF16),
             vmem((8, T, 256), BF16),
             vmem((8, V_ROWS, T), BF16),
             vmem((8, 2 * T, T), F32),
@@ -594,17 +618,18 @@
             vmem((3, 32, D), BF16),
             vmem((3, 32, D), BF16),
             dma((10,)),
-            dma((11,)),
+            dma((12,)),
             dma((11,)),
             dma((4,)),
             dma((5,)),
             dma((6,)),
+            dma((5,)),
             dma((2,)),
             dma((1,)),
             dma((4,)),
             dma((1,)),
             dma((5,)),
-            dma((1,)),
+            dma((2,)),
         ],
         compiler_params=pltpu.CompilerParams(collective_id=0, has_side_effects=True),
     )(

time: 59.7 us -> 59.7 us (level)
  no operation moved by 1% of the time
where the time goes in v4:
time: 59.7 us; the launch traced here: 59.6 us
  Pallas kernels  57.7 us (97%)
  local copies, waits for them, and re-layouts  1.22 us (2%)
  between operations  0.64 us (1%)
    pallas_call x1, Pallas kernels, body(): pl.pallas_call(kernel, out_shape=(vmem((32, D), BF16), vmem((1, T), F32))...  57.7 us
    unnamed x2, local copies, waits for them, and re-layouts  1.22 us

profile of v4, /device:TPU:1, one launch (start us, length us, event | category | flops | bytes accessed | tf_op | source)
XLA Modules:
  0.0 59.6 jit_solution(2065907030874562895)
XLA Ops:
  0.6 57.7 %shard_map.149 = (bf16[32,2048]{1,0:T(8,128)(2,1)S(1)}, f32[1,256]{1,0:T(1,128)S(1)}) custom-call(bf16[256,256]{1,0:T(8,128)(2,1)} %act_hbm.1, f32[1,2048]{1,0:T(1,128)} %bitcast.8, bf16[192,2048]{1,0:T(8,128)(2,1)} %bitcast.5, bf16[64,2048]{1,0:T(8,128)(2,1)} %bitcast.6, bf16[64,2048]{1,0:T(8,128)(2,1)} %bitcast.7, f32[1,512]{1,0:T(1,128)} %bitcast.9, ...), custom_call_target="tpu_custom_call" | custom-call | tf_op jit(solution)/shard_map/pallas_call | solution.py:577
  58.4 0.7 %copy.18 = bf16[32,2048]{1,0:T(8,128)(2,1)} copy(bf16[32,2048]{1,0:T(8,128)(2,1)S(1)} %get-tuple-element.2) | data formatting | bytes 262144
  59.0 0.6 copy.19

commit v5 on v4

--- a/solution.py
+++ b/solution.py
@@ -51,7 +51,7 @@
     table_hbm,
     mixed_ref, lws_ref,
     act_all, gain, lgain, ew, wt, wb, ck, wa_all, wc, table, acc, acc_b, lat_all,
-    q_all, q_cat, kv_all, rope_all, k_cat, vt_all, s_buf, w_buf, r_buf, stats, o_acc, o_send, o_recv, st_recv,
+    q_all, q_cat, kv_all, rope_all, k_cat, vt_all, s_buf, w_buf, r_buf, stats, st_send, o_acc, o_send, o_recv, st_recv,
     halo_out, halo_in, conv_mixed, attended, heads, e_psend, e_precv, e_own, e_xsend, e_xrecv,
     load_sem, sent, a_recv, l_recv, q_recv, kv_recv, r_recv, d_recv, h_recv, ep_recv, ex_recv, w_recv, at_recv,
 ):
@@ -329,6 +329,7 @@
     stats[:, 0:1, :] = jnp.full((8, 1, T), LOW, F32)
     stats[:, 1:8, :] = jnp.zeros((8, 7, T), F32)
     o_acc[...] = jnp.zeros_like(o_acc)
+    st_send[...] = jnp.zeros_like(st_send)
     ones = lax.broadcasted_iota(jnp.int32, (8, V_ROWS - 128, T), 1) == 0
     vt_all[:, 128:V_ROWS, :] = jnp.where(ones, 1.0, 0.0).astype(BF16)
     phase("latent_x")
@@ -413,7 +414,7 @@
     def d_push(offset):
         slot = ring(qa, offset)
         push(o_send.at[slot], o_recv.at[qa], O, d_recv.at[0], q_dev(offset))
-        push(stats.at[slot], st_recv.at[qa], ST, d_recv.at[1], q_dev(offset))
+        push(st_send.at[slot], st_recv.at[qa], ST, d_recv.at[1], q_dev(offset))
 
     def key_step(step, _):
         for s in (1, 2):
@@ -482,10 +483,13 @@
     for d in (3, -3):
         open_keys(ring(ka, d))
     phase("last_keys")
-    for offsets in ((4, 3, 5), (2, 6), (1, 7, 0)):
+    for offsets in ((4,), (3, 5), (2, 6), (1, 7, 0)):
         qs = [ring(qa, offset) for offset in offsets]
         for offset, q, out in zip(offsets, qs, key_blocks((ring(ka, 3), ring(ka, -3)), qs)):
-            stats[q, 1:2, :] = out[128:129]
+            for half in range(2):
+                lanes = slice(128 * half, 128 * half + 128)
+                st_send[q, half : half + 1, :] = stats[q, 0:1, lanes]
+                st_send[q, half + 2 : half + 3, :] = out[128:129, lanes]
             if offset:
                 o_send[q] = out[0:128].astype(BF16)
             else:
@@ -501,16 +505,19 @@
     arrived(st_recv.at[pl.ds(0, 7)], d_recv.at[1])
     arrived(o_recv.at[pl.ds(0, 7)], d_recv.at[0])
     phase("merge")
-    whole_max = stats[qa, 0:1, :]
-    for offset in range(1, 8):
-        whole_max = jnp.maximum(whole_max, st_recv[ring(qa, offset), 0:1, :])
-    weight = jnp.exp2(stats[qa, 0:1, :] - whole_max)
-    whole_sum = stats[qa, 1:2, :] * weight
+    def pair_of(ref, slot, i):
+        return jnp.concatenate([ref[slot, i : i + 1, :], ref[slot, i + 1 : i + 2, :]], axis=1)
+
+    slots = [ring(qa, offset) for offset in range(1, 8)]
+    maxima = [pair_of(st_recv, slot, 0) for slot in slots]
+    own_max = pair_of(st_send, qa, 0)
+    whole_max = functools.reduce(jnp.maximum, maxima, own_max)
+    weight = jnp.exp2(own_max - whole_max)
+    whole_sum = pair_of(st_send, qa, 2) * weight
     whole_out = o_acc[qa, 0:128, :] * weight
-    for offset in range(1, 8):
-        slot = ring(qa, offset)
-        weight = jnp.exp2(st_recv[slot, 0:1, :] - whole_max)
-        whole_sum += st_recv[slot, 1:2, :] * weight
+    for slot, maximum in zip(slots, maxima):
+        weight = jnp.exp2(maximum - whole_max)
+        whole_sum += pair_of(st_recv, slot, 2) * weight
         whole_out += o_recv[slot].astype(F32) * weight
     lws_ref[...] = whole_max * (1.0 / LOG2E) + jnp.log(whole_sum)
     attended[...] = jnp.transpose(whole_out / whole_sum).astype(BF16)
@@ -557,7 +564,7 @@
         (kv_all.at[pl.ds(0, 7)], KV),
         (rope_all.at[pl.ds(0, 7)], R),
         (o_send.at[pl.ds(0, 7)], O),
-        (stats.at[pl.ds(0, 7)], ST),
+        (st_send.at[pl.ds(0, 7)], ST),
         (e_psend, EP),
         (e_xsend, EX),
         (halo_out, H),
@@ -603,10 +610,11 @@
             vmem((8, 2 * T, T), BF16),
             vmem((8, 8, T), F32),
             vmem((8, 8, T), F32),
+            vmem((8, 8, 128), F32),
             vmem((8, V_ROWS, T), F32),
             vmem((8, 128, T), BF16),
             vmem((8, 128, T), BF16),
-            vmem((8, 8, T), F32),
+            vmem((8, 8, 128), F32),
             vmem((2, 8, 128), F32),
             vmem((2, 8, 128), F32),
             vmem((T, 128), BF16),

time: 59.7 us -> 59.1 us (0.990)
  Pallas kernels: 57.7 us -> 57.1 us
where the time goes in v5:
time: 59.1 us; the launch traced here: 59 us
  Pallas kernels  57.1 us (97%)
  local copies, waits for them, and re-layouts  1.22 us (2%)
  between operations  0.64 us (1%)
    pallas_call x1, Pallas kernels, body(): pl.pallas_call(kernel, out_shape=(vmem((32, D), BF16), vmem((1, T), F32))...  57.1 us
    unnamed x2, local copies, waits for them, and re-layouts  1.22 us

profile of v5, /device:TPU:1, one launch (start us, length us, event | category | flops | bytes accessed | tf_op | source)
XLA Modules:
  0.0 59.0 jit_solution(14242422615048664524)
XLA Ops:
  0.6 57.1 %shard_map.149 = (bf16[32,2048]{1,0:T(8,128)(2,1)S(1)}, f32[1,256]{1,0:T(1,128)S(1)}) custom-call(bf16[256,256]{1,0:T(8,128)(2,1)} %act_hbm.1, f32[1,2048]{1,0:T(1,128)} %bitcast.8, bf16[192,2048]{1,0:T(8,128)(2,1)} %bitcast.5, bf16[64,2048]{1,0:T(8,128)(2,1)} %bitcast.6, bf16[64,2048]{1,0:T(8,128)(2,1)} %bitcast.7, f32[1,512]{1,0:T(1,128)} %bitcast.9, ...), custom_call_target="tpu_custom_call" | custom-call | tf_op jit(solution)/shard_map/pallas_call | solution.py:584
  57.8 0.7 %copy.18 = bf16[32,2048]{1,0:T(8,128)(2,1)} copy(bf16[32,2048]{1,0:T(8,128)(2,1)S(1)} %get-tuple-element.2) | data formatting | bytes 262144
  58.4 0.6 copy.19
